TPU v7x, 512 devices: a whole 4x4x16 slice. The times are simulated.
512 devices in a mesh: tp: 16 (over y, x), dp: 32 (over z, core).
Axes of the slice: x: 4, y: 4, z: 16, core: 2. Of those that a mesh axis runs over, the one named last changes fastest.
Arguments:
- hidden_vectors: bfloat16 [192, 4096], P('tp', 'dp'), may hold values from -8 to 8
- live_spans: int32 [96], P('dp'), may hold values from 1 to 2, as said below
- entry_rescale: bfloat16 [2, 4096], P(None, 'dp'), may hold values from 0.099609375 to 1.8984375
- query_weights: bfloat16 [2, 4096, 2048], P(None, 'dp', 'tp'), may hold values from -0.09375 to 0.09375
- address_weights: bfloat16 [2, 4096, 2048], P(None, 'dp', 'tp'), may hold values from -0.09375 to 0.09375
- content_weights: bfloat16 [2, 4096, 2048], P(None, 'dp', 'tp'), may hold values from -0.09375 to 0.09375
- fade_weights: bfloat16 [2, 4096, 2048], P(None, 'dp', 'tp'), may hold values from -0.09375 to 0.09375
- learning_speed_weights: bfloat16 [2, 4096, 2048], P(None, 'dp', 'tp'), may hold values from -0.09375 to 0.09375
- exit_valve_weights: bfloat16 [2, 4096, 2048], P(None, 'dp', 'tp'), may hold values from -0.09375 to 0.09375
- feature_fade_ceiling: float32 [2, 2048], P(None, 'tp'), may hold values from 0.02 to 2
- subspace_rescale: float32 [2, 2048], P(None, 'tp'), may hold values from 0.1 to 1.9
- exit_weights: bfloat16 [2, 2048, 4096], P(None, 'tp', 'dp'), may hold values from -0.125 to 0.125
- memories: float32 [2, 96, 32, 64, 64], P(None, 'dp', 'tp'), may hold values from -6 to 6
- extra_log_fade: float32 [2, 192, 32], P(None, 'dp', 'tp'), may hold values from -0.7 to 0
Outputs:
- hidden_out: bfloat16 [192, 4096], P('tp', 'dp')
- new_states: float32 [2, 96, 32, 64, 64], P(None, 'dp', 'tp')
Inputs may be any that keep to these rules, and one draw needn't show every extreme that they name: `live_spans`: live slots of each sequence; some sequence has 2.
All inputs are finite; a program needn't handle non-finite values.
Results may differ from a plain program's by a relative error of at most 0.0075.
Values may be sent and summed in bfloat16 or wider, within the bound.
A program may use at most 64 MiB of HBM per device.

v0:
```python
import jax
import jax.numpy as jnp
from jax import lax
from jax.sharding import PartitionSpec as P

D = 4096


NORM_EPS = 1e-06
GROUP_EPS = 0.00064


def from_everyone(x, axis):
    size = lax.axis_size(axis)
    return lax.all_to_all(jnp.broadcast_to(x[None], (size, *x.shape)), axis, 0, 0, tiled=True)


def joined_along(tiles, dim):
    tiles = jnp.moveaxis(tiles, 0, dim)
    shape = tiles.shape
    return tiles.reshape(*shape[:dim], shape[dim] * shape[dim + 1], *shape[dim + 2 :])


def gathered_copies(x, axis, dim):
    tiles = from_everyone(x, axis)
    return joined_along(tiles, dim)


def in_blocks(x, dim, size):
    before, after = (x.shape[:dim], x.shape[dim + 1 :])
    return jnp.moveaxis(x.reshape(*before, size, -1, *after), dim, 0)


def sum_at_owner(x, axis, dim):
    tiles = in_blocks(x, dim, lax.axis_size(axis))
    arrived = lax.all_to_all(tiles, axis, split_axis=0, concat_axis=0, tiled=True)
    return arrived.sum(axis=0)


def in_one_piece(arrays, axis, dim, along):
    columns = [a.reshape(*a.shape[:along], -1) for a in arrays]
    both = jnp.concatenate(columns, axis=along)
    result, at, gathered = (sum_at_owner(both, axis, dim), 0, [])
    for a, column in zip(arrays, columns):
        piece = result[..., at : at + column.shape[along]]
        gathered.append(piece.reshape(*piece.shape[:along], *a.shape[along:]))
        at += column.shape[along]
    return tuple(gathered)


def memory_change(
    mapped_vectors,
    live_spans,
    feature_fade_ceiling,
    subspace_rescale,
    running_memory,
    extra_log_fade,
):
    batch_total, subspace_total, subspace_size = (
        running_memory.shape[0],
        running_memory.shape[1],
        running_memory.shape[2],
    )
    position_total = mapped_vectors[0].shape[0] // batch_total

    def by_head(values):
        return values.reshape(batch_total, position_total, subspace_total, subspace_size)

    read_rows, key_rows, value_rows, fade_scores, rate_pre, gate_pre = [
        by_head(v) for v in mapped_vectors
    ]
    fade_multiplier_lines = jnp.exp(
        extra_log_fade.reshape(batch_total, position_total, subspace_total, 1)
        - feature_fade_ceiling.reshape(subspace_total, subspace_size) * jax.nn.sigmoid(fade_scores)
    )
    rate_rows = jax.nn.sigmoid(rate_pre)
    gate_rows = jax.nn.sigmoid(gate_pre)
    unit_keys = key_rows * lax.rsqrt(jnp.sum(key_rows * key_rows, axis=3, keepdims=True) + 1e-06)
    readouts = []
    for position in range(position_total):
        is_live = (live_spans > position).reshape(batch_total, 1, 1, 1)
        unit_now = unit_keys[:, position]
        removed = jnp.einsum(
            "shvk,shk->shv", running_memory, -unit_now, precision=lax.Precision.HIGHEST
        )
        updated = (
            running_memory * fade_multiplier_lines[:, position][:, :, None, :]
            + removed[..., None] * (unit_now * rate_rows[:, position])[:, :, None, :]
            + value_rows[:, position][..., None] * key_rows[:, position][:, :, None, :]
        )
        running_memory = jnp.where(is_live, updated, running_memory)
        readouts.append(
            jnp.einsum(
                "shvk,shk->shv",
                running_memory,
                read_rows[:, position],
                precision=lax.Precision.HIGHEST,
            )
        )
    readout = jnp.stack(readouts, axis=1)
    centered = readout - jnp.mean(readout, axis=3, keepdims=True)
    normed = centered * lax.rsqrt(jnp.mean(centered * centered, axis=3, keepdims=True) + GROUP_EPS)
    normed = normed * subspace_rescale.reshape(subspace_total, subspace_size)
    live_rows = (jnp.arange(position_total)[None, :] < live_spans[:, None]).astype(jnp.float32)[
        :, :, None, None
    ]
    blended_result = (normed * gate_rows * live_rows).astype(jnp.bfloat16)
    return (
        blended_result.reshape(batch_total * position_total, subspace_total * subspace_size),
        running_memory,
    )


def mixer_block(
    rows_here,
    live_spans,
    gain,
    read_w,
    key_w,
    value_w,
    decay_w,
    rate_w,
    gate_w,
    feature_fade_ceiling,
    subspace_rescale,
    out_w,
    running_memory,
    extra_log_fade,
):
    gathered = gathered_copies(rows_here, "tp", 0)
    float_whole = gathered.astype(jnp.float32)
    gained = (float_whole * gain.astype(jnp.float32)).astype(jnp.bfloat16)
    partials = [
        jnp.dot(gained, weight, preferred_element_type=jnp.float32)
        for weight in (read_w, key_w, value_w, decay_w, rate_w, gate_w)
    ]
    partial_squares = jnp.sum(float_whole * float_whole, axis=1)
    summed = in_one_piece(
        (
            partials[0],
            partials[1],
            partials[2],
            partials[3],
            partials[4],
            partials[5],
            partial_squares,
        ),
        "dp",
        0,
        1,
    )
    mapped_vectors = summed[:6]
    squares = summed[6]
    row_scale = lax.rsqrt(squares / D + NORM_EPS)[:, None]
    stretched_vectors = tuple((values * row_scale for values in mapped_vectors))
    blended_result, running_memory = memory_change(
        stretched_vectors,
        live_spans,
        feature_fade_ceiling,
        subspace_rescale,
        running_memory,
        extra_log_fade,
    )
    all_heads = gathered_copies(blended_result, "dp", 0)
    mix_rows = sum_at_owner(jnp.dot(all_heads, out_w, preferred_element_type=jnp.float32), "tp", 0)
    return ((rows_here.astype(jnp.float32) + mix_rows).astype(jnp.bfloat16), running_memory)


def shards(
    hidden_vectors,
    live_spans,
    entry_rescale,
    query_weights,
    address_weights,
    content_weights,
    fade_weights,
    learning_speed_weights,
    exit_valve_weights,
    feature_fade_ceiling,
    subspace_rescale,
    exit_weights,
    memories,
    extra_log_fade,
):
    rows_now = hidden_vectors
    new_states = []
    for layer_ordinal in range(2):
        rows_now, running_memory = mixer_block(
            rows_now,
            live_spans,
            entry_rescale[layer_ordinal],
            query_weights[layer_ordinal],
            address_weights[layer_ordinal],
            content_weights[layer_ordinal],
            fade_weights[layer_ordinal],
            learning_speed_weights[layer_ordinal],
            exit_valve_weights[layer_ordinal],
            feature_fade_ceiling[layer_ordinal],
            subspace_rescale[layer_ordinal],
            exit_weights[layer_ordinal],
            memories[layer_ordinal],
            extra_log_fade[layer_ordinal],
        )
        new_states.append(running_memory)
    return (rows_now, jnp.stack(new_states))


def solution(mesh):
    in_specs = (
        P("tp", "dp"),
        P("dp"),
        P(None, "dp"),
        P(None, "dp", "tp"),
        P(None, "dp", "tp"),
        P(None, "dp", "tp"),
        P(None, "dp", "tp"),
        P(None, "dp", "tp"),
        P(None, "dp", "tp"),
        P(None, "tp"),
        P(None, "tp"),
        P(None, "tp", "dp"),
        P(None, "dp", "tp", None, None),
        P(None, "dp", "tp"),
    )
    out_specs = (P("tp", "dp"), P(None, "dp", "tp", None, None))
    return jax.shard_map(shards, mesh=mesh, in_specs=in_specs, out_specs=out_specs, check_vma=False)
```

profile of v0, /device:TPU:2, one launch (start us, length us, event | category | flops | bytes accessed | tf_op | source)
XLA Modules:
  0.0 226.3 jit_solution(62408614228476302)
XLA Ops:
  0.6 1.3 broadcast_in_dim.32
  2.0 9.3 %all-to-all-start = ((bf16[16,12,128]{2,1,0:T(8,128)(2,1)}), bf16[16,12,128]{2,1,0:T(8,128)(2,1)S(1)}, u32[]{:S(2)}, u32[]{:S(2)}) async-start(bf16[16,12,128]{2,1,0:T(8,128)(2,1)} %broadcast_in_dim.32), calls=%async_computation | async-start | bytes 131072 | tf_op jit(solution)/shard_map/all_to_all | solution.py:15
  11.3 6.3 %all-to-all-done = bf16[16,12,128]{2,1,0:T(8,128)(2,1)S(1)} async-done(((bf16[16,12,128]{2,1,0:T(8,128)(2,1)}), bf16[16,12,128]{2,1,0:T(8,128)(2,1)S(1)}, u32[]{:S(2)}, u32[]{:S(2)}) %all-to-all-start) | async-done | bytes 49184 | tf_op jit(solution)/shard_map/all_to_all | solution.py:15
  17.6 0.1 fusion.25
  17.9 0.4 copy.83
  18.2 0.4 copy-done.2
  18.6 0.1 convolution_dynamic-update-slice_fusion.11
  18.7 0.7 copy-done.3
  19.5 0.1 convolution_dynamic-update-slice_fusion.10
  19.6 0.7 copy-done.4
  20.3 0.1 convolution_dynamic-update-slice_fusion.9
  20.4 0.7 copy-done.5
  21.1 0.1 convolution_dynamic-update-slice_fusion.8
  21.3 0.7 copy-done.6
  22.0 0.1 convolution_dynamic-update-slice_fusion.7
  22.1 0.7 copy-done.7
  22.8 0.1 convolution_dynamic-update-slice_fusion.6
  23.0 1.3 copy.84
  24.3 13.9 %all-to-all-start.1 = ((f32[32,6,769]{2,1,0:T(8,128)}), f32[32,6,769]{2,1,0:T(8,128)S(1)}, u32[]{:S(2)}, u32[]{:S(2)}) async-start(f32[32,6,769]{2,1,0:T(8,128)} %copy.84), calls=%async_computation.1 | async-start | bytes 1835008 | tf_op jit(solution)/shard_map/all_to_all | solution.py:36
  38.3 0.6 copy-done.9
  39.0 0.1 copy.76
  39.1 0.5 copy-done.13
  39.8 0.7 copy-done.12
  40.5 48.1 %all-to-all-done.1 = f32[32,6,769]{2,1,0:T(8,128)S(1)} async-done(((f32[32,6,769]{2,1,0:T(8,128)}), f32[32,6,769]{2,1,0:T(8,128)S(1)}, u32[]{:S(2)}, u32[]{:S(2)}) %all-to-all-start.1) | async-done | bytes 590624 | tf_op jit(solution)/shard_map/all_to_all | solution.py:36
  88.7 0.1 fusion.99
  89.6 0.4 fusion.4
  90.0 0.6 fusion.125
  90.6 0.6 fusion.126
  91.1 0.7 fusion.15
  91.9 0.2 multiply_reduce_fusion.2
  92.3 17.3 %all_to_all.40 = bf16[32,6,128]{2,1,0:T(8,128)(2,1)S(1)} all-to-all(bf16[32,6,128]{2,1,0:T(8,128)(2,1)S(1)} %broadcast_in_dim.34), channel_id=1, replica_groups=mesh['tp'=16,'dp'=32] {'dp'}, dimensions={0} | all-to-all | bytes 98304 | tf_op jit(solution)/shard_map/all_to_all | solution.py:15
  109.7 0.8 copy-done.1
  110.5 0.1 fusion.48
  110.6 11.1 %all_to_all.41 = f32[16,12,128]{2,1,0:T(8,128)S(1)} all-to-all(f32[16,12,128]{2,1,0:T(8,128)S(1)} %fusion.48), channel_id=1, replica_groups=mesh['tp'=16,'dp'=32] {'tp'}, dimensions={0} | all-to-all | bytes 196608 | tf_op jit(solution)/shard_map/all_to_all | solution.py:36
  121.8 0.7 copy-done.8
  122.5 10.7 %all_to_all.42 = bf16[16,12,128]{2,1,0:T(8,128)(2,1)S(1)} all-to-all(bf16[16,12,128]{2,1,0:T(8,128)(2,1)S(1)} %broadcast_in_dim.35), channel_id=1, replica_groups=mesh['tp'=16,'dp'=32] {'tp'}, dimensions={0} | all-to-all | bytes 98304 | tf_op jit(solution)/shard_map/all_to_all | solution.py:15
  133.2 0.1 fusion.27
  133.3 0.1 convolution_dynamic-update-slice_fusion.5
  133.5 0.1 convolution_dynamic-update-slice_fusion.4
  133.6 0.1 convolution_dynamic-update-slice_fusion.3
  133.8 0.1 convolution_dynamic-update-slice_fusion.2
  133.9 0.1 convolution_dynamic-update-slice_fusion.1
  134.0 0.1 convolution_dynamic-update-slice_fusion
  134.3 0.4 copy.95
  134.7 1.3 copy.96
  136.0 3.9 %all-to-all-start.5 = ((f32[32,6,769]{2,1,0:T(8,128)}), f32[32,6,769]{2,1,0:T(8,128)S(1)}, u32[]{:S(2)}, u32[]{:S(2)}) async-start(f32[32,6,769]{2,1,0:T(8,128)} %copy.96), calls=%async_computation.5 | async-start | bytes 1835008 | tf_op jit(solution)/shard_map/all_to_all | solution.py:36
  140.1 0.1 copy.88
  140.2 0.3 add_select_fusion.1
  140.5 50.3 %all-to-all-done.5 = f32[32,6,769]{2,1,0:T(8,128)S(1)} async-done(((f32[32,6,769]{2,1,0:T(8,128)}), f32[32,6,769]{2,1,0:T(8,128)S(1)}, u32[]{:S(2)}, u32[]{:S(2)}) %all-to-all-start.5) | async-done | bytes 590624 | tf_op jit(solution)/shard_map/all_to_all | solution.py:36
  190.9 0.1 fusion.82
  191.6 0.4 fusion
  192.2 0.5 fusion.127
  192.7 0.6 fusion.128
  193.3 0.7 fusion.8
  194.1 0.2 multiply_reduce_fusion
  194.5 0.7 broadcast_in_dim.36
  195.2 3.9 %all-to-all-start.6 = ((bf16[32,6,128]{2,1,0:T(8,128)(2,1)}), bf16[32,6,128]{2,1,0:T(8,128)(2,1)S(1)}, u32[]{:S(2)}, u32[]{:S(2)}) async-start(bf16[32,6,128]{2,1,0:T(8,128)(2,1)} %broadcast_in_dim.36), calls=%async_computation.6 | async-start | bytes 131072 | tf_op jit(solution)/shard_map/all_to_all | solution.py:15
  199.0 0.3 add_select_fusion
  199.3 14.0 %all-to-all-done.6 = bf16[32,6,128]{2,1,0:T(8,128)(2,1)S(1)} async-done(((bf16[32,6,128]{2,1,0:T(8,128)(2,1)}), bf16[32,6,128]{2,1,0:T(8,128)(2,1)S(1)}, u32[]{:S(2)}, u32[]{:S(2)}) %all-to-all-start.6) | async-done | bytes 49184 | tf_op jit(solution)/shard_map/all_to_all | solution.py:15
  213.4 0.8 fusion.40
  214.2 4.8 %all-to-all-start.7 = ((f32[16,12,128]{2,1,0:T(8,128)}), f32[16,12,128]{2,1,0:T(8,128)S(1)}, u32[]{:S(2)}, u32[]{:S(2)}) async-start(f32[16,12,128]{2,1,0:T(8,128)} %fusion.40), calls=%async_computation.7 | async-start | bytes 262144 | tf_op jit(solution)/shard_map/all_to_all | solution.py:36
  218.9 0.8 pad_maximum_fusion
  219.7 5.9 %all-to-all-done.7 = f32[16,12,128]{2,1,0:T(8,128)S(1)} async-done(((f32[16,12,128]{2,1,0:T(8,128)}), f32[16,12,128]{2,1,0:T(8,128)S(1)}, u32[]{:S(2)}, u32[]{:S(2)}) %all-to-all-start.7) | async-done | bytes 98336 | tf_op jit(solution)/shard_map/all_to_all | solution.py:36
  225.7 0.6 add_convert_fusion
  (86 shorter events, 3.3 us)
Async XLA Ops:
  2.0 9.3 %copy-start.10 = (bf16[2,128]{1,0:T(2,128)(2,1)S(1)}, bf16[2,128]{1,0:T(2,128)(2,1)}, u32[]{:S(2)}) copy-start(bf16[2,128]{1,0:T(2,128)(2,1)} %param.16) | copy-start | bytes 1540
  2.0 15.7 %all-to-all-start = ((bf16[16,12,128]{2,1,0:T(8,128)(2,1)}), bf16[16,12,128]{2,1,0:T(8,128)(2,1)S(1)}, u32[]{:S(2)}, u32[]{:S(2)}) async-start(bf16[16,12,128]{2,1,0:T(8,128)(2,1)} %broadcast_in_dim.32), calls=%async_computation | async-start | bytes 131072 | tf_op jit(solution)/shard_map/all_to_all | solution.py:15
  17.8 0.8 copy-start.2
  18.6 0.8 copy-start.3
  19.5 0.8 copy-start.4
  20.3 0.8 copy-start.5
  21.1 0.8 copy-start.6
  22.0 0.8 copy-start.7
  24.3 13.9 %copy-start.11 = (f32[2,128]{1,0:T(2,128)S(1)}, f32[2,128]{1,0:T(2,128)}, u32[]{:S(2)}) copy-start(f32[2,128]{1,0:T(2,128)} %param.23) | copy-start | bytes 3076
  24.3 64.3 %all-to-all-start.1 = ((f32[32,6,769]{2,1,0:T(8,128)}), f32[32,6,769]{2,1,0:T(8,128)S(1)}, u32[]{:S(2)}, u32[]{:S(2)}) async-start(f32[32,6,769]{2,1,0:T(8,128)} %copy.84), calls=%async_computation.1 | async-start | bytes 1835008 | tf_op jit(solution)/shard_map/all_to_all | solution.py:36
  38.2 0.7 copy-start.9
  39.0 0.7 copy-start.13
  39.8 0.7 copy-start.12
  40.5 49.1 %copy-start = (f32[2,3,2,64,64]{4,3,2,1,0:T(8,128)S(1)}, f32[2,3,2,64,64]{4,3,2,1,0:T(8,128)}, u32[]{:S(2)}) copy-start(f32[2,3,2,64,64]{4,3,2,1,0:T(8,128)} %param.26) | copy-start | bytes 589828
  109.6 0.8 copy-start.1
  121.8 0.7 copy-start.8
  136.0 54.8 %all-to-all-start.5 = ((f32[32,6,769]{2,1,0:T(8,128)}), f32[32,6,769]{2,1,0:T(8,128)S(1)}, u32[]{:S(2)}, u32[]{:S(2)}) async-start(f32[32,6,769]{2,1,0:T(8,128)} %copy.96), calls=%async_computation.5 | async-start | bytes 1835008 | tf_op jit(solution)/shard_map/all_to_all | solution.py:36
  195.2 18.2 %all-to-all-start.6 = ((bf16[32,6,128]{2,1,0:T(8,128)(2,1)}), bf16[32,6,128]{2,1,0:T(8,128)(2,1)S(1)}, u32[]{:S(2)}, u32[]{:S(2)}) async-start(bf16[32,6,128]{2,1,0:T(8,128)(2,1)} %broadcast_in_dim.36), calls=%async_computation.6 | async-start | bytes 131072 | tf_op jit(solution)/shard_map/all_to_all | solution.py:15
  214.2 11.5 %all-to-all-start.7 = ((f32[16,12,128]{2,1,0:T(8,128)}), f32[16,12,128]{2,1,0:T(8,128)S(1)}, u32[]{:S(2)}, u32[]{:S(2)}) async-start(f32[16,12,128]{2,1,0:T(8,128)} %fusion.40), calls=%async_computation.7 | async-start | bytes 262144 | tf_op jit(solution)/shard_map/all_to_all | solution.py:36
where the time goes:
time: 227 us; the launch traced here: 226 us
  waiting for transfers between devices  125 us (55%)
  blocking collectives  39.2 us (17%)
  starting transfers between devices  35.7 us (16%)
  local copies, waits for them, and re-layouts  14.6 us (6%)
  matrix products  6.86 us (3%)
  other arithmetic  4.29 us (2%)
    all_to_all x3, waiting for transfers between devices, sum_at_owner(): lax.all_to_all(tiles, axis, split_axis=0, concat_axis=0, tiled=True)  104 us
    all_to_all x2, blocking collectives, from_everyone(): lax.all_to_all(jnp.broadcast_to(x[None], (size, *x.shape)), axis, 0, 0, t...  28 us
    all_to_all x3, starting transfers between devices, sum_at_owner(): lax.all_to_all(tiles, axis, split_axis=0, concat_axis=0, tiled=True)  22.5 us
    all_to_all x2, waiting for transfers between devices, from_everyone(): lax.all_to_all(jnp.broadcast_to(x[None], (size, *x.shape)), axis, 0, 0, t...  20.4 us
    all_to_all x2, starting transfers between devices, from_everyone(): lax.all_to_all(jnp.broadcast_to(x[None], (size, *x.shape)), axis, 0, 0, t...  13.2 us
    all_to_all x1, blocking collectives, sum_at_owner(): lax.all_to_all(tiles, axis, split_axis=0, concat_axis=0, tiled=True)  11.1 us
    unnamed x28, local copies, waits for them, and re-layouts  7.26 us
  transfers between devices with their start and end apart: 5, of which 5 were waited for; matrix products, arithmetic and copies ran while one was open for 1% of the time, Pallas kernels for 0%

commit v1 on v0

v1 whole, which is shorter than its diff:
```python
import jax
import jax.numpy as jnp
from jax import lax
from jax.experimental import pallas as pl
from jax.experimental.pallas import tpu as pltpu
from jax.sharding import PartitionSpec as P

D = 4096
NORM_EPS = 1e-06
GROUP_EPS = 0.00064
TP = 16
NZ = 16
F32 = jnp.float32
BF16 = jnp.bfloat16
MESH = pl.DeviceIdType.MESH


def split_two(x):
    hi = x.astype(BF16)
    lo = (x - hi.astype(F32)).astype(BF16)
    return jnp.concatenate([hi, lo], axis=1)


def kernel(
    x_hbm, live_ref, gain_hbm, wq, wk, wv, wf, wl, we, ceil_hbm, resc_hbm, wo_hbm, mem_hbm, fade_hbm,
    out_hbm, st_hbm,
    xin, xrows, xs, xres, gains, wcat, wout, ceil, resc, fade, mem, packed, states,
    xg, acc, cs, cr, summed, ms, mg, gs, gr, xout,
    load_sem, wsend, wrecv, a_send, a_recv, c_send, c_recv, e_send, e_recv, g_send, g_recv, st_sem, out_sem,
):
    t = lax.axis_index("tp")
    d = lax.axis_index("dp")
    z = d // 2
    c = d % 2
    other = 1 - c

    barrier = pltpu.get_barrier_semaphore()

    def greet_plane(r, carry):
        to = (t + r) % TP
        pl.semaphore_signal(barrier, inc=1, device_id=(to, z * 2), device_id_type=MESH)
        pl.semaphore_signal(barrier, inc=1, device_id=(to, z * 2 + 1), device_id_type=MESH)
        return carry

    def greet_column(r, carry):
        to = (z + r) % NZ
        pl.semaphore_signal(barrier, inc=1, device_id=(t, to * 2 + c), device_id_type=MESH)
        return carry

    lax.fori_loop(1, NZ, greet_column, 0)
    lax.fori_loop(1, TP, greet_plane, 0)
    pl.semaphore_signal(barrier, inc=1, device_id=(t, z * 2 + other), device_id_type=MESH)

    mine = pl.ds(pl.multiple_of(c * 128, 128), 128)
    weights = (wq, wk, wv, wf, wl, we)
    loads = [pltpu.make_async_copy(x_hbm, xin, load_sem.at[0])]
    for p, w in enumerate(weights):
        loads.append(
            pltpu.make_async_copy(w, wcat.at[:, mine, pl.ds(p * 128, 128)], load_sem.at[1 + p])
        )
    loads.append(pltpu.make_async_copy(wo_hbm, wout.at[c], load_sem.at[7]))
    loads.append(pltpu.make_async_copy(gain_hbm, gains.at[c], load_sem.at[8]))
    loads.append(pltpu.make_async_copy(ceil_hbm, ceil, load_sem.at[9]))
    loads.append(pltpu.make_async_copy(resc_hbm, resc, load_sem.at[10]))
    loads.append(pltpu.make_async_copy(mem_hbm, mem, load_sem.at[11]))
    loads.append(pltpu.make_async_copy(fade_hbm, fade, load_sem.at[12]))
    for copy in loads:
        copy.start()

    lane = lax.broadcasted_iota(jnp.int32, (8, 128), 1)
    low_half = lane < 64
    row_at = lax.broadcasted_iota(jnp.int32, (256, 128), 0)
    lane_at = lax.broadcasted_iota(jnp.int32, (256, 128), 1)
    ones_block = jnp.where((row_at % 128) // 64 == lane_at // 64, 1.0, 0.0).astype(BF16)
    own_row = lax.broadcasted_iota(jnp.int32, (64, 128), 0)
    own_lane = lax.broadcasted_iota(jnp.int32, (64, 128), 1)
    diagonal = (own_lane % 64) == own_row

    def head_sum(x):
        return jnp.dot(split_two(x), ones_block, preferred_element_type=F32)

    loads[0].wait()
    xrows[...] = jnp.zeros((16, 128), F32)
    xrows[0:12, :] = xin[...].astype(F32)
    first = xrows[0:8, :]
    second = xrows[6:14, :]
    xres[0] = first
    xres[1] = second
    xs[0, 0] = first.astype(BF16)
    xs[0, 1] = second.astype(BF16)
    for copy in loads[1:]:
        copy.wait()

    pl.semaphore_wait(barrier, 2 * (TP - 1) + NZ)

    def plane_copy(b, to, core):
        return pltpu.make_async_remote_copy(
            src_ref=xs.at[b, core],
            dst_ref=xg.at[b, c * TP + t],
            send_sem=a_send.at[b],
            recv_sem=a_recv.at[b],
            device_id=(to, z * 2 + core),
            device_id_type=MESH,
        )

    def gather_plane(b):
        def step(r, carry):
            to = (t + r) % TP
            plane_copy(b, to, 0).start()
            plane_copy(b, to, 1).start()
            return carry

        lax.fori_loop(1, TP, step, 0)
        plane_copy(b, t, other).start()
        xg[b, c * TP + t] = xs[b, c]

    def swap(src, dst, i):
        return pltpu.make_async_remote_copy(
            src_ref=src,
            dst_ref=dst,
            send_sem=wsend.at[i],
            recv_sem=wrecv.at[i],
            device_id=(t, z * 2 + other),
            device_id_type=MESH,
        )

    gather_plane(0)
    theirs = wcat.at[:, mine, :]
    swaps = [
        swap(gains.at[c], gains.at[c], 0),
        swap(theirs, theirs, 1),
        swap(wout.at[c], wout.at[c], 2),
    ]
    for copy in swaps:
        copy.start()

    for b in range(2):
        for s in range(3):
            packed[b, s] = jnp.concatenate([mem[b, s, 0], mem[b, s, 1]], axis=1)

    def all_of(src, dst, send, recv):
        return pltpu.make_async_remote_copy(
            src_ref=src, dst_ref=dst, send_sem=send, recv_sem=recv,
            device_id=(t, z * 2 + other), device_id_type=MESH,
        )

    for b in range(2):
        if b == 0:
            for copy in swaps:
                copy.wait_recv()
        all_of(xg.at[b, 0:31], xg.at[b, 0:31], a_send.at[b], a_recv.at[b]).wait_recv()

        halves = [xg[b, h * TP : (h + 1) * TP].astype(F32).reshape(128, 128) for h in range(2)]
        gained = jnp.concatenate(
            [
                (halves[h] * gains[h, b : b + 1, :].astype(F32)).astype(BF16)
                for h in range(2)
            ],
            axis=1,
        )
        squares = jnp.sum(halves[0] * halves[0] + halves[1] * halves[1], axis=1, keepdims=True)
        squares = jnp.broadcast_to(squares, (128, 128)).reshape(TP, 8, 128)
        sixteen = lax.broadcasted_iota(jnp.int32, (TP, 3, 128), 2) < 64
        acc[:, 36:40, :] = jnp.zeros((TP, 4, 128), F32)
        acc[:, 36:39, :] = jnp.where(sixteen, squares[:, 0:3], squares[:, 3:6])
        for p in range(6):
            part = jnp.dot(
                gained, wcat[b, :, p * 128 : (p + 1) * 128], preferred_element_type=F32
            )
            acc[:, p * 6 : p * 6 + 6, :] = part.reshape(TP, 8, 128)[:, 0:6]
        cs[b] = acc[...].astype(BF16)

        def reduce_step(i, carry):
            away = (i + 1) // 2
            r = 8 + away * (2 * (i % 2) - 1)
            to = (z + r) % NZ
            pltpu.make_async_remote_copy(
                src_ref=cs.at[b, to],
                dst_ref=cr.at[b, z],
                send_sem=c_send.at[b],
                recv_sem=c_recv.at[b],
                device_id=(t, to * 2 + c),
                device_id_type=MESH,
            ).start()
            return carry

        lax.fori_loop(0, NZ - 1, reduce_step, 0)
        cr[b, z] = cs[b, z]

        row8 = lax.broadcasted_iota(jnp.int32, (8, 128), 0)
        live8 = jnp.zeros((8, 128), jnp.int32)
        for s in range(3):
            live8 = jnp.where(row8 // 2 == s, live_ref[s], live8)
        live_rows = (row8 % 2) < live8
        fade8 = jnp.where(low_half[0:6], fade[b, :, 0:1], fade[b, :, 1:2])

        all_of(cr.at[b, 0:15], cr.at[b, 0:15], c_send.at[b], c_recv.at[b]).wait_recv()
        summed[0:40, :] = jnp.sum(cr[b].astype(F32), axis=0)
        square_rows = summed[36:39, :]
        low_squares = square_rows[:, 0:1]
        high_squares = square_rows[:, 64:65]
        token_squares = jnp.concatenate([low_squares, high_squares], axis=0)
        row_scale = lax.rsqrt(token_squares / D + NORM_EPS)
        read, key, value, decay_pre, rate_pre, gate_pre = [
            summed[p * 6 : p * 6 + 6, :] * row_scale for p in range(6)
        ]
        decay = jnp.exp(fade8 - ceil[b : b + 1, :] * jax.nn.sigmoid(decay_pre))
        rate = jax.nn.sigmoid(rate_pre)
        gate = jax.nn.sigmoid(gate_pre)
        unit = key * lax.rsqrt(head_sum(key * key) + 1e-06)
        unit_rate = unit * rate
        spread = head_sum(
            jnp.concatenate(
                [jnp.where(diagonal, value[i : i + 1, :], 0.0) for i in range(6)], axis=0
            )
        )
        memory = [packed[b, s] for s in range(3)]
        readouts = [None] * 6
        for j in range(2):
            removed = head_sum(
                jnp.concatenate(
                    [memory[s] * unit[2 * s + j : 2 * s + j + 1, :] for s in range(3)], axis=0
                )
            )
            for s in range(3):
                i = 2 * s + j
                updated = (
                    memory[s] * decay[i : i + 1, :]
                    - removed[64 * s : 64 * s + 64] * unit_rate[i : i + 1, :]
                    + spread[64 * i : 64 * i + 64] * key[i : i + 1, :]
                )
                memory[s] = jnp.where(j < live_ref[s], updated, memory[s])
            read_out = head_sum(
                jnp.concatenate(
                    [memory[s] * read[2 * s + j : 2 * s + j + 1, :] for s in range(3)], axis=0
                )
            )
            for s in range(3):
                readouts[2 * s + j] = jnp.sum(
                    jnp.where(diagonal, read_out[64 * s : 64 * s + 64], 0.0), axis=0, keepdims=True
                )
        readout = jnp.concatenate(readouts, axis=0)
        centered = readout - head_sum(readout) * (1.0 / 64.0)
        variance = head_sum(centered * centered) * (1.0 / 64.0)
        normed = centered * lax.rsqrt(variance + GROUP_EPS) * resc[b : b + 1, :]
        mixed = jnp.where(live_rows[0:6], normed * gate, 0.0)
        ms[b] = jnp.concatenate([mixed, jnp.zeros((2, 128), F32)], axis=0).astype(BF16)

        def mixed_step(i, carry):
            away = (i + 1) // 2
            r = 8 + away * (2 * (i % 2) - 1)
            to = (z + r) % NZ
            pltpu.make_async_remote_copy(
                src_ref=ms.at[b],
                dst_ref=mg.at[b, z],
                send_sem=e_send.at[b],
                recv_sem=e_recv.at[b],
                device_id=(t, to * 2 + c),
                device_id_type=MESH,
            ).start()
            return carry

        lax.fori_loop(0, NZ - 1, mixed_step, 0)
        mg[b, z] = ms[b]
        for s in range(3):
            states[b, s, 0] = memory[s][:, 0:64]
            states[b, s, 1] = memory[s][:, 64:128]
        pltpu.make_async_copy(states.at[b], st_hbm.at[b], st_sem.at[b]).start()

        all_of(mg.at[b, 0:15], mg.at[b, 0:15], e_send.at[b], e_recv.at[b]).wait_recv()
        heads = mg[b].astype(F32).reshape(128, 128).astype(BF16)
        for h in range(2):
            part = jnp.dot(heads, wout[h, b], preferred_element_type=F32)
            gs[b, h] = part.reshape(NZ, 8, 128).astype(BF16)

        def owner_copy(to, core):
            return pltpu.make_async_remote_copy(
                src_ref=gs.at[b, core, to],
                dst_ref=gr.at[b, c * TP + t],
                send_sem=g_send.at[b],
                recv_sem=g_recv.at[b],
                device_id=(to, z * 2 + core),
                device_id_type=MESH,
            )

        def owner_step(r, carry):
            to = (t + r) % TP
            owner_copy(to, 0).start()
            owner_copy(to, 1).start()
            return carry

        lax.fori_loop(1, TP, owner_step, 0)
        owner_copy(t, other).start()
        gr[b, c * TP + t] = gs[b, c, t]

        all_of(gr.at[b, 0:31], gr.at[b, 0:31], g_send.at[b], g_recv.at[b]).wait_recv()
        for h in range(2):
            mix = jnp.sum(gr[b, h * TP : (h + 1) * TP].astype(F32), axis=0)
            following = (xres[h] + mix).astype(BF16)
            if b == 0:
                xs[1, h] = following
                xres[h] = following.astype(F32)
            else:
                xrows[6 * h : 6 * h + 6, :] = following.astype(F32)[0:6]
        if b == 0:
            gather_plane(1)
        else:
            xout[...] = xrows[0:12, :].astype(BF16)
            final = pltpu.make_async_copy(xout, out_hbm, out_sem)
            final.start()

    for copy in swaps:
        copy.wait_send()
    for b in range(2):
        pltpu.make_async_copy(states.at[b], st_hbm.at[b], st_sem.at[b]).wait()
        all_of(xg.at[b, 0:31], xg.at[b, 0:31], a_send.at[b], a_recv.at[b]).wait_send()
        all_of(cr.at[b, 0:15], cr.at[b, 0:15], c_send.at[b], c_recv.at[b]).wait_send()
        all_of(mg.at[b, 0:15], mg.at[b, 0:15], e_send.at[b], e_recv.at[b]).wait_send()
        all_of(gr.at[b, 0:31], gr.at[b, 0:31], g_send.at[b], g_recv.at[b]).wait_send()
    final.wait()


def shards(*arrays):
    hbm = pl.BlockSpec(memory_space=pltpu.HBM)
    in_specs = [hbm] * 14
    in_specs[1] = pl.BlockSpec(memory_space=pltpu.SMEM)
    dma = pltpu.SemaphoreType.DMA
    return pl.pallas_call(
        kernel,
        out_shape=(
            jax.ShapeDtypeStruct((12, 128), BF16),
            jax.ShapeDtypeStruct((2, 3, 2, 64, 64), F32),
        ),
        in_specs=in_specs,
        out_specs=(hbm, hbm),
        scratch_shapes=[
            pltpu.VMEM((12, 128), BF16),
            pltpu.VMEM((16, 128), F32),
            pltpu.VMEM((2, 2, 8, 128), BF16),
            pltpu.VMEM((2, 8, 128), F32),
            pltpu.VMEM((2, 2, 128), BF16),
            pltpu.VMEM((2, 256, 768), BF16),
            pltpu.VMEM((2, 2, 128, 128), BF16),
            pltpu.VMEM((2, 128), F32),
            pltpu.VMEM((2, 128), F32),
            pltpu.VMEM((2, 6, 2), F32),
            pltpu.VMEM((2, 3, 2, 64, 64), F32),
            pltpu.VMEM((2, 3, 64, 128), F32),
            pltpu.VMEM((2, 3, 2, 64, 64), F32),
            pltpu.VMEM((2, 32, 8, 128), BF16),
            pltpu.VMEM((16, 40, 128), F32),
            pltpu.VMEM((2, 16, 40, 128), BF16),
            pltpu.VMEM((2, 16, 40, 128), BF16),
            pltpu.VMEM((40, 128), F32),
            pltpu.VMEM((2, 8, 128), BF16),
            pltpu.VMEM((2, 16, 8, 128), BF16),
            pltpu.VMEM((2, 2, 16, 8, 128), BF16),
            pltpu.VMEM((2, 32, 8, 128), BF16),
            pltpu.VMEM((12, 128), BF16),
            dma((13,)),
            dma((3,)),
            dma((3,)),
            dma((2,)),
            dma((2,)),
            dma((2,)),
            dma((2,)),
            dma((2,)),
            dma((2,)),
            dma((2,)),
            dma((2,)),
            dma((2,)),
            dma,
        ],
        compiler_params=pltpu.CompilerParams(collective_id=0, has_side_effects=True),
    )(*arrays)


def solution(mesh):
    in_specs = (
        P("tp", "dp"),
        P("dp"),
        P(None, "dp"),
        P(None, "dp", "tp"),
        P(None, "dp", "tp"),
        P(None, "dp", "tp"),
        P(None, "dp", "tp"),
        P(None, "dp", "tp"),
        P(None, "dp", "tp"),
        P(None, "tp"),
        P(None, "tp"),
        P(None, "tp", "dp"),
        P(None, "dp", "tp", None, None),
        P(None, "dp", "tp"),
    )
    out_specs = (P("tp", "dp"), P(None, "dp", "tp", None, None))
    return jax.shard_map(shards, mesh=mesh, in_specs=in_specs, out_specs=out_specs, check_vma=False)
```

time: 227 us -> 80.6 us (0.36)
  the two profiles are of different devices: /device:TPU:2 before, /device:TPU:1 now
where the time goes in v1:
time: 80.6 us; the launch traced here: 80.4 us
  Pallas kernels  75.4 us (94%)
  local copies, waits for them, and re-layouts  4.4 us (5%)
    pallas_call x1, Pallas kernels, shards(): pl.pallas_call(kernel, out_shape=(jax.ShapeDtypeStruct((12, 128), BF16),...  75.4 us
    unnamed x3, local copies, waits for them, and re-layouts  4.4 us

profile of v1, /device:TPU:1, one launch (start us, length us, event | category | flops | bytes accessed | tf_op | source)
XLA Modules:
  0.0 80.4 jit_solution(6769168407980672568)
XLA Ops:
  0.6 1.4 %copy.16.fade_hbm = f32[2,6,2]{2,1,0:T(8,128)} copy(f32[2,6,2]{1,2,0:T(2,128)} %param.27) | data formatting | bytes 192 | tf_op args[13]
  2.0 75.4 %shard_map.149 = (bf16[12,128]{1,0:T(8,128)(2,1)}, f32[2,3,2,64,64]{4,3,2,1,0:T(8,128)}) custom-call(bf16[12,128]{1,0:T(8,128)(2,1)} %x_hbm.1, s32[3]{0:T(128)} %live_ref.1, bf16[2,128]{1,0:T(2,128)(2,1)} %gain_hbm.1, bf16[2,128,128]{2,1,0:T(8,128)(2,1)} %wq.1, bf16[2,128,128]{2,1,0:T(8,128)(2,1)} %wk.1, bf16[2,128,128]{2,1,0:T(8,128)(2,1)} %wv.1, ...), custom_call_target="tpu_custom_call" | custom-call | tf_op jit(solution)/shard_map/pallas_call | solution.py:328
  77.4 1.3 %copy.19 = bf16[12,128]{1,0:T(8,128)(2,1)} copy(bf16[12,128]{1,0:T(8,128)(2,1)} %get-tuple-element.4) | data formatting | bytes 6144
  78.6 1.8 %copy.20 = f32[2,3,2,64,64]{4,3,2,1,0:T(8,128)} copy(f32[2,3,2,64,64]{4,3,2,1,0:T(8,128)} %get-tuple-element.5) | data formatting | bytes 393216

commit v2 on v1

v2 whole, which is shorter than its diff:
```python
import jax
import jax.numpy as jnp
from jax import lax
from jax.experimental import pallas as pl
from jax.experimental.pallas import tpu as pltpu
from jax.sharding import PartitionSpec as P

D = 4096
NORM_EPS = 1e-06
GROUP_EPS = 0.00064
TP = 16
NZ = 16
WIDTH = 2048
F32 = jnp.float32
BF16 = jnp.bfloat16
MESH = pl.DeviceIdType.MESH


def split_two(x):
    hi = x.astype(BF16)
    lo = (x - hi.astype(F32)).astype(BF16)
    return jnp.concatenate([hi, lo], axis=1)


def kernel(
    x_hbm, live_ref, gain_hbm, wq, wk, wv, wf, wl, we, ceil_hbm, resc_hbm, wo_hbm, mem_hbm, fade_hbm,
    out_hbm, st_hbm,
    xin, xrows, xs, gains, wcat, wall0, wall1, ceil, resc, fade, mem, packed, states,
    xg, acc, cs, cr, summed, ms, mg, xw, x1s, xr1, fin, xout,
    load_sem, swap_send, swap_recv, a_send, a_recv, c_send, c_recv, e_send, e_recv, f_send, f_recv,
    w_send, w_recv, l_send, l_recv, st_sem, out_sem,
):
    t = lax.axis_index("tp")
    d = lax.axis_index("dp")
    z = d // 2
    c = d % 2
    other = 1 - c
    away = (t + NZ - z) % NZ
    past_half = away // 9
    slot_here = (1 - past_half) * (2 * away - (away + 15) // 16) + past_half * (32 - 2 * away)

    barrier = pltpu.get_barrier_semaphore()

    def greet_plane(r, carry):
        to = (t + r) % TP
        pl.semaphore_signal(barrier, inc=1, device_id=(to, z * 2), device_id_type=MESH)
        pl.semaphore_signal(barrier, inc=1, device_id=(to, z * 2 + 1), device_id_type=MESH)
        return carry

    def greet_column(r, carry):
        to = (z + r) % NZ
        pl.semaphore_signal(barrier, inc=1, device_id=(t, to * 2 + c), device_id_type=MESH)
        return carry

    lax.fori_loop(1, NZ, greet_column, 0)
    lax.fori_loop(1, TP, greet_plane, 0)
    pl.semaphore_signal(barrier, inc=1, device_id=(t, z * 2 + other), device_id_type=MESH)

    mine = pl.ds(pl.multiple_of(c * 128, 128), 128)
    weights = (wq, wk, wv, wf, wl, we)
    loads = [pltpu.make_async_copy(x_hbm, xin, load_sem.at[0])]
    for p, w in enumerate(weights):
        loads.append(
            pltpu.make_async_copy(w, wcat.at[:, mine, pl.ds(p * 128, 128)], load_sem.at[1 + p])
        )
    loads.append(pltpu.make_async_copy(wo_hbm.at[0], wall0.at[t, :, mine], load_sem.at[7]))
    loads.append(pltpu.make_async_copy(wo_hbm.at[1], wall1.at[t], load_sem.at[13]))
    loads.append(pltpu.make_async_copy(gain_hbm, gains.at[c], load_sem.at[8]))
    loads.append(pltpu.make_async_copy(ceil_hbm, ceil, load_sem.at[9]))
    loads.append(pltpu.make_async_copy(resc_hbm, resc, load_sem.at[10]))
    loads.append(pltpu.make_async_copy(mem_hbm, mem, load_sem.at[11]))
    loads.append(pltpu.make_async_copy(fade_hbm, fade, load_sem.at[12]))
    for copy in loads:
        copy.start()

    lane = lax.broadcasted_iota(jnp.int32, (8, 128), 1)
    low_half = lane < 64
    row_at = lax.broadcasted_iota(jnp.int32, (256, 128), 0)
    lane_at = lax.broadcasted_iota(jnp.int32, (256, 128), 1)
    ones_block = jnp.where((row_at % 128) // 64 == lane_at // 64, 1.0, 0.0).astype(BF16)
    own_row = lax.broadcasted_iota(jnp.int32, (64, 128), 0)
    own_lane = lax.broadcasted_iota(jnp.int32, (64, 128), 1)
    diagonal = (own_lane % 64) == own_row

    def head_sum(x):
        return jnp.dot(split_two(x), ones_block, preferred_element_type=F32)

    loads[0].wait()
    xrows[...] = jnp.zeros((16, 128), F32)
    xrows[0:12, :] = xin[...].astype(F32)
    first = xrows[0:8, :]
    second = xrows[6:14, :]
    xs[0] = first.astype(BF16)
    xs[1] = second.astype(BF16)
    for copy in loads[1:]:
        copy.wait()

    pl.semaphore_wait(barrier, 2 * (TP - 1) + NZ)

    def remote(src, dst, send, recv, to_t, to_z, to_c):
        return pltpu.make_async_remote_copy(
            src_ref=src, dst_ref=dst, send_sem=send, recv_sem=recv,
            device_id=(to_t, to_z * 2 + to_c), device_id_type=MESH,
        )

    def to_sibling(src, i):
        return remote(src, src, swap_send.at[i], swap_recv.at[i], t, z, other)

    def row_copy(to, core):
        return remote(
            xs.at[core], xg.at[c, slot_here], a_send, a_recv, to, z, core
        )

    def row_step(r, carry):
        to = (t + r) % TP
        row_copy(to, 0).start()
        row_copy(to, 1).start()
        return carry

    lax.fori_loop(1, TP, row_step, 0)
    row_copy(t, other).start()
    xg[c, slot_here] = xs[c]

    swaps = [
        to_sibling(gains.at[c], 0),
        to_sibling(wcat.at[0, mine, :], 1),
        to_sibling(wcat.at[1, mine, :], 2),
        to_sibling(wall0.at[:, :, mine], 3),
    ]
    swaps[0].start()
    swaps[1].start()

    def exit_step(r, carry):
        mine_here = wall0.at[t, :, mine]
        remote(mine_here, mine_here, w_send.at[0], w_recv.at[0], (t + r) % TP, z, c).start()
        return carry

    lax.fori_loop(1, TP, exit_step, 0)

    def exit_step_last(r, carry):
        remote(wall1.at[t], wall1.at[t], w_send.at[1], w_recv.at[1], (t + r) % TP, z, c).start()
        return carry

    for b in range(2):
        for s in range(3):
            packed[b, s] = jnp.concatenate([mem[b, s, 0], mem[b, s, 1]], axis=1)

    fade_columns = jnp.transpose(jnp.concatenate([fade[0], fade[1], jnp.zeros((4, 6), F32)], axis=0))

    def all_of(ref, send, recv):
        return remote(ref, ref, send, recv, t, z, other)

    def column(start, first, last):
        if last == 8:
            start((z + 8) % NZ, 15, 15)

        def step(i, carry):
            dist = min(last, 7) - i
            start((z + dist) % NZ, 2 * dist - 1, 2 * dist)
            start((z + NZ - dist) % NZ, 2 * dist, 2 * dist - 1)
            return carry

        lax.fori_loop(0, min(last, 7) - first + 1, step, 0)

    def project(b, rows, lo, hi):
        count = (hi - lo) * 8
        gained = jnp.concatenate(
            [(rows[h] * gains[h, b : b + 1, :].astype(F32)).astype(BF16) for h in range(2)],
            axis=1,
        )
        squares = jnp.sum(rows[0] * rows[0] + rows[1] * rows[1], axis=1, keepdims=True)
        squares = jnp.broadcast_to(squares, (count, 128)).reshape(hi - lo, 8, 128)
        lower = lax.broadcasted_iota(jnp.int32, (hi - lo, 3, 128), 2) < 64
        acc[lo:hi, 36:40, :] = jnp.zeros((hi - lo, 4, 128), F32)
        acc[lo:hi, 36:39, :] = jnp.where(lower, squares[:, 0:3], squares[:, 3:6])
        for p in range(6):
            part = jnp.dot(
                gained, wcat[b, :, p * 128 : (p + 1) * 128], preferred_element_type=F32
            )
            acc[lo:hi, p * 6 : p * 6 + 6, :] = part.reshape(hi - lo, 8, 128)[:, 0:6]
        cs[b, lo:hi] = acc[lo:hi].astype(BF16)

    def send_partials(b, first, last):
        def start(to, here, there):
            remote(cs.at[b, here], cr.at[b, z], c_send.at[b], c_recv.at[b], t, to, c).start()

        column(start, first, last)

    groups = ((0, 7, 1, 3), (7, 13, 4, 6), (13, 16, 7, 8))
    for b in range(2):
        if b == 0:
            swaps[0].wait_recv()
            swaps[1].wait_recv()
            all_of(fin.at[0:31], a_send, a_recv).wait_recv()
            rows = [xg[h].astype(F32).reshape(128, 128) for h in range(2)]
            project(0, rows, 0, 16)
            send_partials(0, 1, 8)
            lax.fori_loop(1, TP, exit_step_last, 0)
        else:
            swaps[2].wait_recv()
            swaps[3].wait_recv()
            for g, (lo, hi, first, last) in enumerate(groups):
                count = (hi - lo) * 8
                all_of(xw.at[0:15, lo:hi], f_send.at[g], f_recv.at[g]).wait_recv()
                heads = jnp.concatenate(
                    [xw[i, lo:hi].astype(F32).reshape(count, 128).astype(BF16) for i in range(TP)],
                    axis=1,
                )
                mix = jnp.dot(
                    heads, wall0[...].reshape(WIDTH, 256), preferred_element_type=F32
                )
                rows = []
                for h in range(2):
                    before = xg[h, lo:hi].astype(F32).reshape(count, 128)
                    after = (before + mix[:, 128 * h : 128 * h + 128]).astype(BF16).astype(F32)
                    x1s[h, lo:hi] = after.reshape(hi - lo, 8, 128).astype(BF16)
                    rows.append(after)
                project(1, rows, lo, hi)
                send_partials(1, first, last)
            residual = remote(
                x1s.at[other, slot_here], xr1, l_send, l_recv, t, z, other
            )
            residual.start()
        own = cs[b, 0]
        cr[b, z] = own

        row8 = lax.broadcasted_iota(jnp.int32, (8, 128), 0)
        live8 = jnp.zeros((8, 128), jnp.int32)
        for s in range(3):
            live8 = jnp.where(row8 // 2 == s, live_ref[s], live8)
        live_rows = (row8 % 2) < live8
        fade8 = jnp.where(low_half[0:6], fade_columns[:, 2 * b : 2 * b + 1], fade_columns[:, 2 * b + 1 : 2 * b + 2])

        all_of(cr.at[b, 0:15], c_send.at[b], c_recv.at[b]).wait_recv()
        summed[0:40, :] = jnp.sum(cr[b].astype(F32), axis=0)
        square_rows = summed[36:39, :]
        low_squares = square_rows[:, 0:1]
        high_squares = square_rows[:, 64:65]
        token_squares = jnp.concatenate([low_squares, high_squares], axis=0)
        row_scale = lax.rsqrt(token_squares / D + NORM_EPS)
        read, key, value, decay_pre, rate_pre, gate_pre = [
            summed[p * 6 : p * 6 + 6, :] * row_scale for p in range(6)
        ]
        decay = jnp.exp(fade8 - ceil[b : b + 1, :] * jax.nn.sigmoid(decay_pre))
        rate = jax.nn.sigmoid(rate_pre)
        gate = jax.nn.sigmoid(gate_pre)
        unit = key * lax.rsqrt(head_sum(key * key) + 1e-06)
        unit_rate = unit * rate
        spread = head_sum(
            jnp.concatenate(
                [jnp.where(diagonal, value[i : i + 1, :], 0.0) for i in range(6)], axis=0
            )
        )
        memory = [packed[b, s] for s in range(3)]
        readouts = [None] * 6
        for j in range(2):
            removed = head_sum(
                jnp.concatenate(
                    [memory[s] * unit[2 * s + j : 2 * s + j + 1, :] for s in range(3)], axis=0
                )
            )
            for s in range(3):
                i = 2 * s + j
                updated = (
                    memory[s] * decay[i : i + 1, :]
                    - removed[64 * s : 64 * s + 64] * unit_rate[i : i + 1, :]
                    + spread[64 * i : 64 * i + 64] * key[i : i + 1, :]
                )
                memory[s] = jnp.where(j < live_ref[s], updated, memory[s])
            read_out = head_sum(
                jnp.concatenate(
                    [memory[s] * read[2 * s + j : 2 * s + j + 1, :] for s in range(3)], axis=0
                )
            )
            for s in range(3):
                readouts[2 * s + j] = jnp.sum(
                    jnp.where(diagonal, read_out[64 * s : 64 * s + 64], 0.0), axis=0, keepdims=True
                )
        readout = jnp.concatenate(readouts, axis=0)
        centered = readout - head_sum(readout) * (1.0 / 64.0)
        variance = head_sum(centered * centered) * (1.0 / 64.0)
        normed = centered * lax.rsqrt(variance + GROUP_EPS) * resc[b : b + 1, :]
        mixed = jnp.where(live_rows[0:6], normed * gate, 0.0)
        ms[b] = jnp.concatenate([mixed, jnp.zeros((2, 128), F32)], axis=0).astype(BF16)

        if b == 0:
            for g in (2, 1, 0):
                lo, hi, first, last = groups[g]

                def start(to, here, there):
                    remote(
                        ms.at[0], mg.at[there], e_send.at[g], e_recv.at[g], t, to, c
                    ).start()

                column(start, first, last)
            mg[0] = ms[0]
            all_of(wall0.at[0:15, :, mine], w_send.at[0], w_recv.at[0]).wait_recv()
            swaps[3].start()
            swaps[2].start()
        else:
            def start_both(to, here, there):
                for core in range(2):
                    remote(
                        ms.at[1], fin.at[c * TP + t], e_send.at[3], e_recv.at[3], z, to, core
                    ).start()

            column(start_both, 1, 8)

            @pl.when(t == z)
            def _():
                remote(
                    ms.at[1], fin.at[c * TP + t], e_send.at[3], e_recv.at[3], z, z, other
                ).start()
                fin[c * TP + t] = ms[1]

            @pl.when(t != z)
            def _():
                for core in range(2):
                    remote(
                        ms.at[1], fin.at[c * TP + t], e_send.at[3], e_recv.at[3], z, z, core
                    ).start()

        for s in range(3):
            states[b, s, 0] = memory[s][:, 0:64]
            states[b, s, 1] = memory[s][:, 64:128]
        pltpu.make_async_copy(states.at[b], st_hbm.at[b], st_sem.at[b]).start()

        if b == 0:
            for g, (lo, hi, first, last) in enumerate(groups):
                arriving = mg.at[max(lo, 1) : hi]
                all_of(arriving, e_send.at[g], e_recv.at[g]).wait_recv()

                def forward(r, carry):
                    remote(
                        mg.at[lo:hi], xw.at[t, lo:hi], f_send.at[g], f_recv.at[g],
                        (t + r) % TP, z, c,
                    ).start()
                    return carry

                lax.fori_loop(1, TP, forward, 0)
                xw[t, lo:hi] = mg[lo:hi]

    all_of(wall1.at[0:15], w_send.at[1], w_recv.at[1]).wait_recv()
    residual.wait_recv()

    @pl.when(t == z)
    def _():
        all_of(fin.at[0:31], e_send.at[3], e_recv.at[3]).wait_recv()

    @pl.when(t != z)
    def _():
        all_of(fin, e_send.at[3], e_recv.at[3]).wait_recv()

    heads = jnp.concatenate(
        [
            jnp.concatenate([fin[i].astype(F32), fin[TP + i].astype(F32)], axis=0).astype(BF16)
            for i in range(TP)
        ],
        axis=1,
    )
    mix = jnp.dot(heads, wall1[...].reshape(WIDTH, 128), preferred_element_type=F32)
    here_rows = x1s[c, slot_here].astype(F32)
    there_rows = xr1[...].astype(F32)
    core = jnp.full((8, 128), c, jnp.int32)
    xrows[0:6, :] = (jnp.where(core == 0, here_rows, there_rows) + mix[0:8])[0:6]
    xrows[6:12, :] = (jnp.where(core == 0, there_rows, here_rows) + mix[8:16])[0:6]
    xout[...] = xrows[0:12, :].astype(BF16)
    final = pltpu.make_async_copy(xout, out_hbm, out_sem)
    final.start()

    for copy in swaps:
        copy.wait_send()
    residual.wait_send()
    all_of(fin.at[0:31], a_send, a_recv).wait_send()
    all_of(wall0.at[0:15, :, mine], w_send.at[0], w_recv.at[0]).wait_send()
    all_of(wall1.at[0:15], w_send.at[1], w_recv.at[1]).wait_send()
    for b in range(2):
        pltpu.make_async_copy(states.at[b], st_hbm.at[b], st_sem.at[b]).wait()
        all_of(cr.at[b, 0:15], c_send.at[b], c_recv.at[b]).wait_send()
    for g, (lo, hi, first, last) in enumerate(groups):
        all_of(mg.at[max(lo, 1) : hi], e_send.at[g], e_recv.at[g]).wait_send()
        all_of(xw.at[0:15, lo:hi], f_send.at[g], f_recv.at[g]).wait_send()

    @pl.when(t == z)
    def _():
        all_of(fin.at[0:31], e_send.at[3], e_recv.at[3]).wait_send()

    @pl.when(t != z)
    def _():
        all_of(fin, e_send.at[3], e_recv.at[3]).wait_send()

    final.wait()


def shards(*arrays):
    arrays = arrays[:13] + (jnp.transpose(arrays[13], (0, 2, 1)),)
    hbm = pl.BlockSpec(memory_space=pltpu.HBM)
    in_specs = [hbm] * 14
    in_specs[1] = pl.BlockSpec(memory_space=pltpu.SMEM)
    dma = pltpu.SemaphoreType.DMA
    return pl.pallas_call(
        kernel,
        out_shape=(
            jax.ShapeDtypeStruct((12, 128), BF16),
            jax.ShapeDtypeStruct((2, 3, 2, 64, 64), F32),
        ),
        in_specs=in_specs,
        out_specs=(hbm, hbm),
        scratch_shapes=[
            pltpu.VMEM((12, 128), BF16),
            pltpu.VMEM((16, 128), F32),
            pltpu.VMEM((2, 8, 128), BF16),
            pltpu.VMEM((2, 2, 128), BF16),
            pltpu.VMEM((2, 256, 768), BF16),
            pltpu.VMEM((16, 128, 256), BF16),
            pltpu.VMEM((16, 128, 128), BF16),
            pltpu.VMEM((2, 128), F32),
            pltpu.VMEM((2, 128), F32),
            pltpu.VMEM((2, 2, 6), F32),
            pltpu.VMEM((2, 3, 2, 64, 64), F32),
            pltpu.VMEM((2, 3, 64, 128), F32),
            pltpu.VMEM((2, 3, 2, 64, 64), F32),
            pltpu.VMEM((2, 16, 8, 128), BF16),
            pltpu.VMEM((16, 40, 128), F32),
            pltpu.VMEM((2, 16, 40, 128), BF16),
            pltpu.VMEM((2, 16, 40, 128), BF16),
            pltpu.VMEM((40, 128), F32),
            pltpu.VMEM((2, 8, 128), BF16),
            pltpu.VMEM((16, 8, 128), BF16),
            pltpu.VMEM((16, 16, 8, 128), BF16),
            pltpu.VMEM((2, 16, 8, 128), BF16),
            pltpu.VMEM((8, 128), BF16),
            pltpu.VMEM((32, 8, 128), BF16),
            pltpu.VMEM((12, 128), BF16),
            dma((14,)),
            dma((4,)),
            dma((4,)),
            dma,
            dma,
            dma((2,)),
            dma((2,)),
            dma((4,)),
            dma((4,)),
            dma((3,)),
            dma((3,)),
            dma((2,)),
            dma((2,)),
            dma,
            dma,
            dma((2,)),
            dma,
        ],
        compiler_params=pltpu.CompilerParams(collective_id=0, has_side_effects=True),
    )(*arrays)


def solution(mesh):
    in_specs = (
        P("tp", "dp"),
        P("dp"),
        P(None, "dp"),
        P(None, "dp", "tp"),
        P(None, "dp", "tp"),
        P(None, "dp", "tp"),
        P(None, "dp", "tp"),
        P(None, "dp", "tp"),
        P(None, "dp", "tp"),
        P(None, "tp"),
        P(None, "tp"),
        P(None, "tp", "dp"),
        P(None, "dp", "tp", None, None),
        P(None, "dp", "tp"),
    )
    out_specs = (P("tp", "dp"), P(None, "dp", "tp", None, None))
    return jax.shard_map(shards, mesh=mesh, in_specs=in_specs, out_specs=out_specs, check_vma=False)
```

time: 80.6 us -> 70.7 us (0.88)
  the two profiles are of different devices: /device:TPU:1 before, /device:TPU:17 now
where the time goes in v2:
time: 70.7 us; the launch traced here: 70.5 us
  Pallas kernels  66.8 us (94%)
  local copies, waits for them, and re-layouts  3.03 us (4%)
    pallas_call x1, Pallas kernels, shards(): pl.pallas_call(kernel, out_shape=(jax.ShapeDtypeStruct((12, 128), BF16),...  66.8 us
    unnamed x2, local copies, waits for them, and re-layouts  3.03 us

profile of v2, /device:TPU:17, one launch (start us, length us, event | category | flops | bytes accessed | tf_op | source)
XLA Modules:
  0.0 70.5 jit_solution(6557973691853378480)
XLA Ops:
  0.6 66.8 %shard_map.149 = (bf16[12,128]{1,0:T(8,128)(2,1)}, f32[2,3,2,64,64]{4,3,2,1,0:T(8,128)}) custom-call(bf16[12,128]{1,0:T(8,128)(2,1)} %x_hbm.1, s32[3]{0:T(128)} %live_ref.1, bf16[2,128]{1,0:T(2,128)(2,1)} %gain_hbm.1, bf16[2,128,128]{2,1,0:T(8,128)(2,1)} %wq.1, bf16[2,128,128]{2,1,0:T(8,128)(2,1)} %wk.1, bf16[2,128,128]{2,1,0:T(8,128)(2,1)} %wv.1, ...), custom_call_target="tpu_custom_call" | custom-call | tf_op jit(solution)/shard_map/pallas_call | solution.py:401
  67.5 1.3 %copy.18 = bf16[12,128]{1,0:T(8,128)(2,1)} copy(bf16[12,128]{1,0:T(8,128)(2,1)} %get-tuple-element.4) | data formatting | bytes 6144
  68.7 1.8 %copy.19 = f32[2,3,2,64,64]{4,3,2,1,0:T(8,128)} copy(f32[2,3,2,64,64]{4,3,2,1,0:T(8,128)} %get-tuple-element.5) | data formatting | bytes 393216

commit v3 on v2

--- a/solution.py
+++ b/solution.py
@@ -10,6 +10,7 @@
 GROUP_EPS = 0.00064
 TP = 16
 NZ = 16
+NEAR = 4
 WIDTH = 2048
 F32 = jnp.float32
 BF16 = jnp.bfloat16
@@ -23,12 +24,12 @@
 
 
 def kernel(
-    x_hbm, live_ref, gain_hbm, wq, wk, wv, wf, wl, we, ceil_hbm, resc_hbm, wo_hbm, mem_hbm, fade_hbm,
-    out_hbm, st_hbm,
-    xin, xrows, xs, gains, wcat, wall0, wall1, ceil, resc, fade, mem, packed, states,
-    xg, acc, cs, cr, summed, ms, mg, xw, x1s, xr1, fin, xout,
+    x_hbm, live_hbm, gain_hbm, wq, wk, wv, wf, wl, we, ceil_hbm, resc_hbm, wo_hbm, mem_hbm, fade_hbm,
+    out_ref, states,
+    live_ref, xin, xrows, xs, gains, wcat, wall0, wall1, ceil, resc, fade, mem, packed,
+    xg, acc, cs, cr, summed, ms, mg, xw, x1s, xr1, fin,
     load_sem, swap_send, swap_recv, a_send, a_recv, c_send, c_recv, e_send, e_recv, f_send, f_recv,
-    w_send, w_recv, l_send, l_recv, st_sem, out_sem,
+    w_send, w_recv, l_send, l_recv, far_sem,
 ):
     t = lax.axis_index("tp")
     d = lax.axis_index("dp")
@@ -48,17 +49,20 @@
         return carry
 
     def greet_column(r, carry):
-        to = (z + r) % NZ
-        pl.semaphore_signal(barrier, inc=1, device_id=(t, to * 2 + c), device_id_type=MESH)
+        for to in ((z + r) % NZ, (z + NZ - r) % NZ):
+            pl.semaphore_signal(barrier, inc=1, device_id=(t, to * 2 + c), device_id_type=MESH)
         return carry
 
-    lax.fori_loop(1, NZ, greet_column, 0)
+    lax.fori_loop(1, NEAR + 1, greet_column, 0)
     lax.fori_loop(1, TP, greet_plane, 0)
     pl.semaphore_signal(barrier, inc=1, device_id=(t, z * 2 + other), device_id_type=MESH)
 
     mine = pl.ds(pl.multiple_of(c * 128, 128), 128)
     weights = (wq, wk, wv, wf, wl, we)
-    loads = [pltpu.make_async_copy(x_hbm, xin, load_sem.at[0])]
+    loads = [
+        pltpu.make_async_copy(x_hbm, xin, load_sem.at[0]),
+        pltpu.make_async_copy(live_hbm, live_ref, load_sem.at[14]),
+    ]
     for p, w in enumerate(weights):
         loads.append(
             pltpu.make_async_copy(w, wcat.at[:, mine, pl.ds(p * 128, 128)], load_sem.at[1 + p])
@@ -95,7 +99,7 @@
     for copy in loads[1:]:
         copy.wait()
 
-    pl.semaphore_wait(barrier, 2 * (TP - 1) + NZ)
+    pl.semaphore_wait(barrier, 2 * (TP - 1) + 1 + 2 * NEAR)
 
     def remote(src, dst, send, recv, to_t, to_z, to_c):
         return pltpu.make_async_remote_copy(
@@ -119,6 +123,8 @@
 
     lax.fori_loop(1, TP, row_step, 0)
     row_copy(t, other).start()
+    for to in ((z + NEAR) % NZ, (z + NZ - NEAR) % NZ):
+        pl.semaphore_signal(far_sem, inc=1, device_id=(t, to * 2 + c), device_id_type=MESH)
     xg[c, slot_here] = xs[c]
 
     swaps = [
@@ -134,8 +140,6 @@
         mine_here = wall0.at[t, :, mine]
         remote(mine_here, mine_here, w_send.at[0], w_recv.at[0], (t + r) % TP, z, c).start()
         return carry
-
-    lax.fori_loop(1, TP, exit_step, 0)
 
     def exit_step_last(r, carry):
         remote(wall1.at[t], wall1.at[t], w_send.at[1], w_recv.at[1], (t + r) % TP, z, c).start()
@@ -194,8 +198,9 @@
             all_of(fin.at[0:31], a_send, a_recv).wait_recv()
             rows = [xg[h].astype(F32).reshape(128, 128) for h in range(2)]
             project(0, rows, 0, 16)
+            pl.semaphore_wait(far_sem, 2)
             send_partials(0, 1, 8)
-            lax.fori_loop(1, TP, exit_step_last, 0)
+            lax.fori_loop(1, TP, exit_step, 0)
         else:
             swaps[2].wait_recv()
             swaps[3].wait_recv()
@@ -221,6 +226,7 @@
                 x1s.at[other, slot_here], xr1, l_send, l_recv, t, z, other
             )
             residual.start()
+            lax.fori_loop(1, TP, exit_step_last, 0)
         own = cs[b, 0]
         cr[b, z] = own
 
@@ -323,7 +329,6 @@
         for s in range(3):
             states[b, s, 0] = memory[s][:, 0:64]
             states[b, s, 1] = memory[s][:, 64:128]
-        pltpu.make_async_copy(states.at[b], st_hbm.at[b], st_sem.at[b]).start()
 
         if b == 0:
             for g, (lo, hi, first, last) in enumerate(groups):
@@ -364,9 +369,7 @@
     core = jnp.full((8, 128), c, jnp.int32)
     xrows[0:6, :] = (jnp.where(core == 0, here_rows, there_rows) + mix[0:8])[0:6]
     xrows[6:12, :] = (jnp.where(core == 0, there_rows, here_rows) + mix[8:16])[0:6]
-    xout[...] = xrows[0:12, :].astype(BF16)
-    final = pltpu.make_async_copy(xout, out_hbm, out_sem)
-    final.start()
+    out_ref[...] = xrows[0:12, :].astype(BF16)
 
     for copy in swaps:
         copy.wait_send()
@@ -375,7 +378,6 @@
     all_of(wall0.at[0:15, :, mine], w_send.at[0], w_recv.at[0]).wait_send()
     all_of(wall1.at[0:15], w_send.at[1], w_recv.at[1]).wait_send()
     for b in range(2):
-        pltpu.make_async_copy(states.at[b], st_hbm.at[b], st_sem.at[b]).wait()
         all_of(cr.at[b, 0:15], c_send.at[b], c_recv.at[b]).wait_send()
     for g, (lo, hi, first, last) in enumerate(groups):
         all_of(mg.at[max(lo, 1) : hi], e_send.at[g], e_recv.at[g]).wait_send()
@@ -389,24 +391,23 @@
     def _():
         all_of(fin, e_send.at[3], e_recv.at[3]).wait_send()
 
-    final.wait()
-
 
 def shards(*arrays):
     arrays = arrays[:13] + (jnp.transpose(arrays[13], (0, 2, 1)),)
+    arrays = tuple(pltpu.with_memory_space_constraint(a, pltpu.HBM) for a in arrays)
     hbm = pl.BlockSpec(memory_space=pltpu.HBM)
     in_specs = [hbm] * 14
-    in_specs[1] = pl.BlockSpec(memory_space=pltpu.SMEM)
     dma = pltpu.SemaphoreType.DMA
     return pl.pallas_call(
         kernel,
         out_shape=(
-            jax.ShapeDtypeStruct((12, 128), BF16),
-            jax.ShapeDtypeStruct((2, 3, 2, 64, 64), F32),
+            pltpu.VMEM((12, 128), BF16),
+            pltpu.VMEM((2, 3, 2, 64, 64), F32),
         ),
         in_specs=in_specs,
-        out_specs=(hbm, hbm),
+        out_specs=(pl.BlockSpec(memory_space=pltpu.VMEM),) * 2,
         scratch_shapes=[
+            pltpu.SMEM((3,), jnp.int32),
             pltpu.VMEM((12, 128), BF16),
             pltpu.VMEM((16, 128), F32),
             pltpu.VMEM((2, 8, 128), BF16),
@@ -419,7 +420,6 @@
             pltpu.VMEM((2, 2, 6), F32),
             pltpu.VMEM((2, 3, 2, 64, 64), F32),
             pltpu.VMEM((2, 3, 64, 128), F32),
-            pltpu.VMEM((2, 3, 2, 64, 64), F32),
             pltpu.VMEM((2, 16, 8, 128), BF16),
             pltpu.VMEM((16, 40, 128), F32),
             pltpu.VMEM((2, 16, 40, 128), BF16),
@@ -431,8 +431,7 @@
             pltpu.VMEM((2, 16, 8, 128), BF16),
             pltpu.VMEM((8, 128), BF16),
             pltpu.VMEM((32, 8, 128), BF16),
-            pltpu.VMEM((12, 128), BF16),
-            dma((14,)),
+            dma((15,)),
             dma((4,)),
             dma((4,)),
             dma,
@@ -447,10 +446,9 @@
             dma((2,)),
             dma,
             dma,
-            dma((2,)),
-            dma,
+            pltpu.SemaphoreType.REGULAR,
         ],
-        compiler_params=pltpu.CompilerParams(collective_id=0, has_side_effects=True),
+        compiler_params=pltpu.CompilerParams(collective_id=0, has_side_effects=True, vmem_limit_bytes=24 * 1024 * 1024),
     )(*arrays)
 
 

time: 70.7 us -> 62.4 us (0.88)
  Pallas kernels: 66.8 us -> 60.3 us
  local copies, waits for them, and re-layouts: 3.03 us -> 1.34 us
    pallas_call x1, Pallas kernels: 66.8 us -> 60.3 us  [shards(): pl.pallas_call(kernel, out_shape=(pltpu.VMEM((12, 128), BF16), pltpu.VMEM...]
    unnamed x2, local copies, waits for them, and re-layouts: 3.03 us -> 1.34 us
where the time goes in v3:
time: 62.4 us; the launch traced here: 62.3 us
  Pallas kernels  60.3 us (97%)
  local copies, waits for them, and re-layouts  1.34 us (2%)
  between operations  0.64 us (1%)
    pallas_call x1, Pallas kernels, shards(): pl.pallas_call(kernel, out_shape=(pltpu.VMEM((12, 128), BF16), pltpu.VMEM...  60.3 us
    unnamed x2, local copies, waits for them, and re-layouts  1.34 us

profile of v3, /device:TPU:17, one launch (start us, length us, event | category | flops | bytes accessed | tf_op | source)
XLA Modules:
  0.0 62.3 jit_solution(9224510409115066596)
XLA Ops:
  0.6 60.3 %shard_map.149 = (bf16[12,128]{1,0:T(8,128)(2,1)S(1)}, f32[2,3,2,64,64]{4,3,2,1,0:T(8,128)S(1)}) custom-call(bf16[12,128]{1,0:T(8,128)(2,1)} %x_hbm.1, s32[3]{0:T(128)} %live_hbm.1, bf16[2,128]{1,0:T(2,128)(2,1)} %gain_hbm.1, bf16[2,128,128]{2,1,0:T(8,128)(2,1)} %wq.1, bf16[2,128,128]{2,1,0:T(8,128)(2,1)} %wk.1, bf16[2,128,128]{2,1,0:T(8,128)(2,1)} %wv.1, ...), custom_call_target="tpu_custom_call" | custom-call | tf_op jit(solution)/shard_map/pallas_call | solution.py:401
  61.0 0.6 copy.18
  61.5 0.7 %copy.19 = f32[2,3,2,64,64]{4,3,2,1,0:T(8,128)} copy(f32[2,3,2,64,64]{4,3,2,1,0:T(8,128)S(1)} %get-tuple-element.3) | data formatting | bytes 393216

commit v4 on v3

--- a/solution.py
+++ b/solution.py
@@ -10,7 +10,11 @@
 GROUP_EPS = 0.00064
 TP = 16
 NZ = 16
-NEAR = 4
+SIDE = 4
+AROUND = sorted(
+    ((i, j) for i in range(SIDE) for j in range(SIDE) if i + j > 0),
+    key=lambda at: -min(at[0], SIDE - at[0]) - min(at[1], SIDE - at[1]),
+)
 WIDTH = 2048
 F32 = jnp.float32
 BF16 = jnp.bfloat16
@@ -27,7 +31,7 @@
     x_hbm, live_hbm, gain_hbm, wq, wk, wv, wf, wl, we, ceil_hbm, resc_hbm, wo_hbm, mem_hbm, fade_hbm,
     out_ref, states,
     live_ref, xin, xrows, xs, gains, wcat, wall0, wall1, ceil, resc, fade, mem, packed,
-    xg, acc, cs, cr, summed, ms, mg, xw, x1s, xr1, fin,
+    xa, xg, acc, cs, cr, summed, ms, mg, xw, x1s, xr1, fin,
     load_sem, swap_send, swap_recv, a_send, a_recv, c_send, c_recv, e_send, e_recv, f_send, f_recv,
     w_send, w_recv, l_send, l_recv, far_sem,
 ):
@@ -42,19 +46,23 @@
 
     barrier = pltpu.get_barrier_semaphore()
 
-    def greet_plane(r, carry):
-        to = (t + r) % TP
-        pl.semaphore_signal(barrier, inc=1, device_id=(to, z * 2), device_id_type=MESH)
-        pl.semaphore_signal(barrier, inc=1, device_id=(to, z * 2 + 1), device_id_type=MESH)
-        return carry
-
-    def greet_column(r, carry):
-        for to in ((z + r) % NZ, (z + NZ - r) % NZ):
-            pl.semaphore_signal(barrier, inc=1, device_id=(t, to * 2 + c), device_id_type=MESH)
-        return carry
-
-    lax.fori_loop(1, NEAR + 1, greet_column, 0)
-    lax.fori_loop(1, TP, greet_plane, 0)
+    y = t // SIDE
+    x = t % SIDE
+
+    def in_plane(up, right):
+        return ((y + up) % SIDE) * SIDE + (x + right) % SIDE
+
+    def greet(to_t, to_z, to_c):
+        pl.semaphore_signal(
+            barrier, inc=1, device_id=(to_t, to_z * 2 + to_c), device_id_type=MESH
+        )
+
+    for r in (2, 1, 3):
+        greet(in_plane(0, r), z, 0)
+        greet(in_plane(0, r), z, 1)
+        greet(in_plane(r, 0), z, c)
+    for r in (2, NZ - 2, 1, NZ - 1):
+        greet(t, (z + r) % NZ, c)
     pl.semaphore_signal(barrier, inc=1, device_id=(t, z * 2 + other), device_id_type=MESH)
 
     mine = pl.ds(pl.multiple_of(c * 128, 128), 128)
@@ -99,7 +107,7 @@
     for copy in loads[1:]:
         copy.wait()
 
-    pl.semaphore_wait(barrier, 2 * (TP - 1) + 1 + 2 * NEAR)
+    pl.semaphore_wait(barrier, 14)
 
     def remote(src, dst, send, recv, to_t, to_z, to_c):
         return pltpu.make_async_remote_copy(
@@ -111,21 +119,18 @@
         return remote(src, src, swap_send.at[i], swap_recv.at[i], t, z, other)
 
     def row_copy(to, core):
-        return remote(
-            xs.at[core], xg.at[c, slot_here], a_send, a_recv, to, z, core
-        )
-
-    def row_step(r, carry):
-        to = (t + r) % TP
-        row_copy(to, 0).start()
-        row_copy(to, 1).start()
-        return carry
-
-    lax.fori_loop(1, TP, row_step, 0)
+        return remote(xs.at[core], xa.at[c, t], a_send.at[0], a_recv.at[0], to, z, core)
+
+    def tell(sem, r):
+        for to in ((z + r) % NZ, (z + NZ - r) % NZ):
+            pl.semaphore_signal(sem, inc=1, device_id=(t, to * 2 + c), device_id_type=MESH)
+
+    for r in (2, 1, 3):
+        row_copy(in_plane(0, r), 0).start()
+        row_copy(in_plane(0, r), 1).start()
     row_copy(t, other).start()
-    for to in ((z + NEAR) % NZ, (z + NZ - NEAR) % NZ):
-        pl.semaphore_signal(far_sem, inc=1, device_id=(t, to * 2 + c), device_id_type=MESH)
-    xg[c, slot_here] = xs[c]
+    tell(far_sem.at[0], 2)
+    xa[c, t] = xs[c]
 
     swaps = [
         to_sibling(gains.at[c], 0),
@@ -193,12 +198,28 @@
     groups = ((0, 7, 1, 3), (7, 13, 4, 6), (13, 16, 7, 8))
     for b in range(2):
         if b == 0:
+            pl.semaphore_wait(far_sem.at[0], 2)
+            tell(far_sem.at[1], 4)
+            all_of(fin.at[0:7], a_send.at[0], a_recv.at[0]).wait_recv()
+            line = xa.at[:, pl.ds(y * SIDE, SIDE)]
+            for r in (2, 1, 3):
+                remote(
+                    line, line, a_send.at[1], a_recv.at[1], in_plane(r, 0), z, c
+                ).start()
             swaps[0].wait_recv()
             swaps[1].wait_recv()
-            all_of(fin.at[0:31], a_send, a_recv).wait_recv()
-            rows = [xg[h].astype(F32).reshape(128, 128) for h in range(2)]
+            all_of(fin.at[0:24], a_send.at[1], a_recv.at[1]).wait_recv()
+            order = [z] + [
+                (z + ((k + 1) // 2 if k % 2 else NZ - k // 2)) % NZ for k in range(1, NZ)
+            ]
+            rows = []
+            for h in range(2):
+                tiles = [xa[h, at] for at in order]
+                for k in range(NZ):
+                    xg[h, k] = tiles[k]
+                rows.append(jnp.concatenate([tile.astype(F32) for tile in tiles], axis=0))
             project(0, rows, 0, 16)
-            pl.semaphore_wait(far_sem, 2)
+            pl.semaphore_wait(far_sem.at[1], 2)
             send_partials(0, 1, 8)
             lax.fori_loop(1, TP, exit_step, 0)
         else:
@@ -335,14 +356,11 @@
                 arriving = mg.at[max(lo, 1) : hi]
                 all_of(arriving, e_send.at[g], e_recv.at[g]).wait_recv()
 
-                def forward(r, carry):
+                for up, right in AROUND:
                     remote(
                         mg.at[lo:hi], xw.at[t, lo:hi], f_send.at[g], f_recv.at[g],
-                        (t + r) % TP, z, c,
+                        in_plane(up, right), z, c,
                     ).start()
-                    return carry
-
-                lax.fori_loop(1, TP, forward, 0)
                 xw[t, lo:hi] = mg[lo:hi]
 
     all_of(wall1.at[0:15], w_send.at[1], w_recv.at[1]).wait_recv()
@@ -374,7 +392,8 @@
     for copy in swaps:
         copy.wait_send()
     residual.wait_send()
-    all_of(fin.at[0:31], a_send, a_recv).wait_send()
+    all_of(fin.at[0:7], a_send.at[0], a_recv.at[0]).wait_send()
+    all_of(fin.at[0:24], a_send.at[1], a_recv.at[1]).wait_send()
     all_of(wall0.at[0:15, :, mine], w_send.at[0], w_recv.at[0]).wait_send()
     all_of(wall1.at[0:15], w_send.at[1], w_recv.at[1]).wait_send()
     for b in range(2):
@@ -421,6 +440,7 @@
             pltpu.VMEM((2, 3, 2, 64, 64), F32),
             pltpu.VMEM((2, 3, 64, 128), F32),
             pltpu.VMEM((2, 16, 8, 128), BF16),
+            pltpu.VMEM((2, 16, 8, 128), BF16),
             pltpu.VMEM((16, 40, 128), F32),
             pltpu.VMEM((2, 16, 40, 128), BF16),
             pltpu.VMEM((2, 16, 40, 128), BF16),
@@ -434,8 +454,8 @@
             dma((15,)),
             dma((4,)),
             dma((4,)),
-            dma,
-            dma,
+            dma((2,)),
+            dma((2,)),
             dma((2,)),
             dma((2,)),
             dma((4,)),
@@ -446,7 +466,7 @@
             dma((2,)),
             dma,
             dma,
-            pltpu.SemaphoreType.REGULAR,
+            pltpu.SemaphoreType.REGULAR((2,)),
         ],
         compiler_params=pltpu.CompilerParams(collective_id=0, has_side_effects=True, vmem_limit_bytes=24 * 1024 * 1024),
     )(*arrays)

time: 62.4 us -> 64.5 us (1.034)
  Pallas kernels: 60.3 us -> 62.4 us
    pallas_call x1, Pallas kernels: 60.3 us -> 62.4 us  [shards(): pl.pallas_call(kernel, out_shape=(pltpu.VMEM((12, 128), BF16), pltpu.VMEM...]
where the time goes in v4:
time: 64.5 us; the launch traced here: 64.4 us
  Pallas kernels  62.4 us (97%)
  local copies, waits for them, and re-layouts  1.34 us (2%)
    pallas_call x1, Pallas kernels, shards(): pl.pallas_call(kernel, out_shape=(pltpu.VMEM((12, 128), BF16), pltpu.VMEM...  62.4 us
    unnamed x2, local copies, waits for them, and re-layouts  1.34 us

profile of v4, /device:TPU:17, one launch (start us, length us, event | category | flops | bytes accessed | tf_op | source)
XLA Modules:
  0.0 64.4 jit_solution(7777027322154974448)
XLA Ops:
  0.6 62.4 %shard_map.149 = (bf16[12,128]{1,0:T(8,128)(2,1)S(1)}, f32[2,3,2,64,64]{4,3,2,1,0:T(8,128)S(1)}) custom-call(bf16[12,128]{1,0:T(8,128)(2,1)} %x_hbm.1, s32[3]{0:T(128)} %live_hbm.1, bf16[2,128]{1,0:T(2,128)(2,1)} %gain_hbm.1, bf16[2,128,128]{2,1,0:T(8,128)(2,1)} %wq.1, bf16[2,128,128]{2,1,0:T(8,128)(2,1)} %wk.1, bf16[2,128,128]{2,1,0:T(8,128)(2,1)} %wv.1, ...), custom_call_target="tpu_custom_call" | custom-call | tf_op jit(solution)/shard_map/pallas_call | solution.py:420
  63.0 0.6 copy.18
  63.6 0.7 %copy.19 = f32[2,3,2,64,64]{4,3,2,1,0:T(8,128)} copy(f32[2,3,2,64,64]{4,3,2,1,0:T(8,128)S(1)} %get-tuple-element.3) | data formatting | bytes 393216

commit v5 on v4

--- a/solution.py
+++ b/solution.py
@@ -46,6 +46,8 @@
 
     barrier = pltpu.get_barrier_semaphore()
 
+    load_rows = pltpu.make_async_copy(x_hbm, xin, load_sem.at[0])
+    load_rows.start()
     y = t // SIDE
     x = t % SIDE
 
@@ -67,10 +69,7 @@
 
     mine = pl.ds(pl.multiple_of(c * 128, 128), 128)
     weights = (wq, wk, wv, wf, wl, we)
-    loads = [
-        pltpu.make_async_copy(x_hbm, xin, load_sem.at[0]),
-        pltpu.make_async_copy(live_hbm, live_ref, load_sem.at[14]),
-    ]
+    loads = [pltpu.make_async_copy(live_hbm, live_ref, load_sem.at[14])]
     for p, w in enumerate(weights):
         loads.append(
             pltpu.make_async_copy(w, wcat.at[:, mine, pl.ds(p * 128, 128)], load_sem.at[1 + p])
@@ -97,16 +96,13 @@
     def head_sum(x):
         return jnp.dot(split_two(x), ones_block, preferred_element_type=F32)
 
-    loads[0].wait()
+    load_rows.wait()
     xrows[...] = jnp.zeros((16, 128), F32)
     xrows[0:12, :] = xin[...].astype(F32)
     first = xrows[0:8, :]
     second = xrows[6:14, :]
     xs[0] = first.astype(BF16)
     xs[1] = second.astype(BF16)
-    for copy in loads[1:]:
-        copy.wait()
-
     pl.semaphore_wait(barrier, 14)
 
     def remote(src, dst, send, recv, to_t, to_z, to_c):
@@ -138,6 +134,8 @@
         to_sibling(wcat.at[1, mine, :], 2),
         to_sibling(wall0.at[:, :, mine], 3),
     ]
+    for copy in loads:
+        copy.wait()
     swaps[0].start()
     swaps[1].start()
 
@@ -271,8 +269,7 @@
         decay = jnp.exp(fade8 - ceil[b : b + 1, :] * jax.nn.sigmoid(decay_pre))
         rate = jax.nn.sigmoid(rate_pre)
         gate = jax.nn.sigmoid(gate_pre)
-        unit = key * lax.rsqrt(head_sum(key * key) + 1e-06)
-        unit_rate = unit * rate
+        removal = key * rate / (head_sum(key * key) + 1e-06)
         spread = head_sum(
             jnp.concatenate(
                 [jnp.where(diagonal, value[i : i + 1, :], 0.0) for i in range(6)], axis=0
@@ -280,17 +277,18 @@
         )
         memory = [packed[b, s] for s in range(3)]
         readouts = [None] * 6
+        spreads = [None] * 6
         for j in range(2):
             removed = head_sum(
                 jnp.concatenate(
-                    [memory[s] * unit[2 * s + j : 2 * s + j + 1, :] for s in range(3)], axis=0
+                    [memory[s] * key[2 * s + j : 2 * s + j + 1, :] for s in range(3)], axis=0
                 )
             )
             for s in range(3):
                 i = 2 * s + j
                 updated = (
                     memory[s] * decay[i : i + 1, :]
-                    - removed[64 * s : 64 * s + 64] * unit_rate[i : i + 1, :]
+                    - removed[64 * s : 64 * s + 64] * removal[i : i + 1, :]
                     + spread[64 * i : 64 * i + 64] * key[i : i + 1, :]
                 )
                 memory[s] = jnp.where(j < live_ref[s], updated, memory[s])
@@ -300,12 +298,14 @@
                 )
             )
             for s in range(3):
+                here = read_out[64 * s : 64 * s + 64]
+                here = here - jnp.sum(here, axis=0, keepdims=True) * (1.0 / 64.0)
+                spreads[2 * s + j] = jnp.sum(here * here, axis=0, keepdims=True)
                 readouts[2 * s + j] = jnp.sum(
-                    jnp.where(diagonal, read_out[64 * s : 64 * s + 64], 0.0), axis=0, keepdims=True
-                )
-        readout = jnp.concatenate(readouts, axis=0)
-        centered = readout - head_sum(readout) * (1.0 / 64.0)
-        variance = head_sum(centered * centered) * (1.0 / 64.0)
+                    jnp.where(diagonal, here, 0.0), axis=0, keepdims=True
+                )
+        variance = jnp.concatenate(spreads, axis=0) * (1.0 / 64.0)
+        centered = jnp.concatenate(readouts, axis=0)
         normed = centered * lax.rsqrt(variance + GROUP_EPS) * resc[b : b + 1, :]
         mixed = jnp.where(live_rows[0:6], normed * gate, 0.0)
         ms[b] = jnp.concatenate([mixed, jnp.zeros((2, 128), F32)], axis=0).astype(BF16)

time: 64.5 us -> 63.9 us (level)
  no operation moved by 1% of the time
where the time goes in v5:
time: 63.9 us; the launch traced here: 63.8 us
  Pallas kernels  61.8 us (97%)
  local copies, waits for them, and re-layouts  1.34 us (2%)
  between operations  0.64 us (1%)
    pallas_call x1, Pallas kernels, shards(): pl.pallas_call(kernel, out_shape=(pltpu.VMEM((12, 128), BF16), pltpu.VMEM...  61.8 us
    unnamed x2, local copies, waits for them, and re-layouts  1.34 us

profile of v5, /device:TPU:17, one launch (start us, length us, event | category | flops | bytes accessed | tf_op | source)
XLA Modules:
  0.0 63.8 jit_solution(17968945969545377321)
XLA Ops:
  0.6 61.8 %shard_map.149 = (bf16[12,128]{1,0:T(8,128)(2,1)S(1)}, f32[2,3,2,64,64]{4,3,2,1,0:T(8,128)S(1)}) custom-call(bf16[12,128]{1,0:T(8,128)(2,1)} %x_hbm.1, s32[3]{0:T(128)} %live_hbm.1, bf16[2,128]{1,0:T(2,128)(2,1)} %gain_hbm.1, bf16[2,128,128]{2,1,0:T(8,128)(2,1)} %wq.1, bf16[2,128,128]{2,1,0:T(8,128)(2,1)} %wk.1, bf16[2,128,128]{2,1,0:T(8,128)(2,1)} %wv.1, ...), custom_call_target="tpu_custom_call" | custom-call | tf_op jit(solution)/shard_map/pallas_call | solution.py:420
  62.5 0.6 copy.18
  63.1 0.7 %copy.19 = f32[2,3,2,64,64]{4,3,2,1,0:T(8,128)} copy(f32[2,3,2,64,64]{4,3,2,1,0:T(8,128)S(1)} %get-tuple-element.3) | data formatting | bytes 393216

commit v6 on v5

--- a/solution.py
+++ b/solution.py
@@ -31,7 +31,7 @@
     x_hbm, live_hbm, gain_hbm, wq, wk, wv, wf, wl, we, ceil_hbm, resc_hbm, wo_hbm, mem_hbm, fade_hbm,
     out_ref, states,
     live_ref, xin, xrows, xs, gains, wcat, wall0, wall1, ceil, resc, fade, mem, packed,
-    xa, xg, acc, cs, cr, summed, ms, mg, xw, x1s, xr1, fin,
+    xa, xb, xg, acc, cs, cr, summed, ms, mg, xw, x1s, xr1, fin,
     load_sem, swap_send, swap_recv, a_send, a_recv, c_send, c_recv, e_send, e_recv, f_send, f_recv,
     w_send, w_recv, l_send, l_recv, far_sem,
 ):
@@ -62,9 +62,10 @@
     for r in (2, 1, 3):
         greet(in_plane(0, r), z, 0)
         greet(in_plane(0, r), z, 1)
-        greet(in_plane(r, 0), z, c)
+        greet(in_plane(r, 0), z, other)
     for r in (2, NZ - 2, 1, NZ - 1):
-        greet(t, (z + r) % NZ, c)
+        greet(t, (z + r) % NZ, 0)
+        greet(t, (z + r) % NZ, 1)
     pl.semaphore_signal(barrier, inc=1, device_id=(t, z * 2 + other), device_id_type=MESH)
 
     mine = pl.ds(pl.multiple_of(c * 128, 128), 128)
@@ -103,7 +104,7 @@
     second = xrows[6:14, :]
     xs[0] = first.astype(BF16)
     xs[1] = second.astype(BF16)
-    pl.semaphore_wait(barrier, 14)
+    pl.semaphore_wait(barrier, 18)
 
     def remote(src, dst, send, recv, to_t, to_z, to_c):
         return pltpu.make_async_remote_copy(
@@ -157,7 +158,7 @@
     def all_of(ref, send, recv):
         return remote(ref, ref, send, recv, t, z, other)
 
-    def column(start, first, last):
+    def column(start, first, last, whole=True):
         if last == 8:
             start((z + 8) % NZ, 15, 15)
 
@@ -168,6 +169,8 @@
             return carry
 
         lax.fori_loop(0, min(last, 7) - first + 1, step, 0)
+        if first == 1 and whole:
+            start(z, 0, 0)
 
     def project(b, rows, lo, hi):
         count = (hi - lo) * 8
@@ -189,7 +192,9 @@
 
     def send_partials(b, first, last):
         def start(to, here, there):
-            remote(cs.at[b, here], cr.at[b, z], c_send.at[b], c_recv.at[b], t, to, c).start()
+            remote(
+                cs.at[b, here], cr.at[b, z], c_send.at[b], c_recv.at[b], t, to, other
+            ).start()
 
         column(start, first, last)
 
@@ -200,19 +205,20 @@
             tell(far_sem.at[1], 4)
             all_of(fin.at[0:7], a_send.at[0], a_recv.at[0]).wait_recv()
             line = xa.at[:, pl.ds(y * SIDE, SIDE)]
-            for r in (2, 1, 3):
+            there = xb.at[:, pl.ds(y * SIDE, SIDE)]
+            for r in (2, 1, 3, 0):
                 remote(
-                    line, line, a_send.at[1], a_recv.at[1], in_plane(r, 0), z, c
+                    line, there, a_send.at[1], a_recv.at[1], in_plane(r, 0), z, other
                 ).start()
             swaps[0].wait_recv()
             swaps[1].wait_recv()
-            all_of(fin.at[0:24], a_send.at[1], a_recv.at[1]).wait_recv()
+            all_of(fin, a_send.at[1], a_recv.at[1]).wait_recv()
             order = [z] + [
                 (z + ((k + 1) // 2 if k % 2 else NZ - k // 2)) % NZ for k in range(1, NZ)
             ]
             rows = []
             for h in range(2):
-                tiles = [xa[h, at] for at in order]
+                tiles = [xb[h, at] for at in order]
                 for k in range(NZ):
                     xg[h, k] = tiles[k]
                 rows.append(jnp.concatenate([tile.astype(F32) for tile in tiles], axis=0))
@@ -246,9 +252,6 @@
             )
             residual.start()
             lax.fori_loop(1, TP, exit_step_last, 0)
-        own = cs[b, 0]
-        cr[b, z] = own
-
         row8 = lax.broadcasted_iota(jnp.int32, (8, 128), 0)
         live8 = jnp.zeros((8, 128), jnp.int32)
         for s in range(3):
@@ -256,7 +259,7 @@
         live_rows = (row8 % 2) < live8
         fade8 = jnp.where(low_half[0:6], fade_columns[:, 2 * b : 2 * b + 1], fade_columns[:, 2 * b + 1 : 2 * b + 2])
 
-        all_of(cr.at[b, 0:15], c_send.at[b], c_recv.at[b]).wait_recv()
+        all_of(cr.at[b], c_send.at[b], c_recv.at[b]).wait_recv()
         summed[0:40, :] = jnp.sum(cr[b].astype(F32), axis=0)
         square_rows = summed[36:39, :]
         low_squares = square_rows[:, 0:1]
@@ -316,11 +319,10 @@
 
                 def start(to, here, there):
                     remote(
-                        ms.at[0], mg.at[there], e_send.at[g], e_recv.at[g], t, to, c
+                        ms.at[0], mg.at[there], e_send.at[g], e_recv.at[g], t, to, other
                     ).start()
 
                 column(start, first, last)
-            mg[0] = ms[0]
             all_of(wall0.at[0:15, :, mine], w_send.at[0], w_recv.at[0]).wait_recv()
             swaps[3].start()
             swaps[2].start()
@@ -331,7 +333,7 @@
                         ms.at[1], fin.at[c * TP + t], e_send.at[3], e_recv.at[3], z, to, core
                     ).start()
 
-            column(start_both, 1, 8)
+            column(start_both, 1, 8, False)
 
             @pl.when(t == z)
             def _():
@@ -353,7 +355,7 @@
 
         if b == 0:
             for g, (lo, hi, first, last) in enumerate(groups):
-                arriving = mg.at[max(lo, 1) : hi]
+                arriving = mg.at[lo:hi]
                 all_of(arriving, e_send.at[g], e_recv.at[g]).wait_recv()
 
                 for up, right in AROUND:
@@ -385,21 +387,21 @@
     here_rows = x1s[c, slot_here].astype(F32)
     there_rows = xr1[...].astype(F32)
     core = jnp.full((8, 128), c, jnp.int32)
-    xrows[0:6, :] = (jnp.where(core == 0, here_rows, there_rows) + mix[0:8])[0:6]
-    xrows[6:12, :] = (jnp.where(core == 0, there_rows, here_rows) + mix[8:16])[0:6]
+    xrows[0:6, :] = (jnp.where(core == 0, there_rows, here_rows) + mix[0:8])[0:6]
+    xrows[6:12, :] = (jnp.where(core == 0, here_rows, there_rows) + mix[8:16])[0:6]
     out_ref[...] = xrows[0:12, :].astype(BF16)
 
     for copy in swaps:
         copy.wait_send()
     residual.wait_send()
     all_of(fin.at[0:7], a_send.at[0], a_recv.at[0]).wait_send()
-    all_of(fin.at[0:24], a_send.at[1], a_recv.at[1]).wait_send()
+    all_of(fin, a_send.at[1], a_recv.at[1]).wait_send()
     all_of(wall0.at[0:15, :, mine], w_send.at[0], w_recv.at[0]).wait_send()
     all_of(wall1.at[0:15], w_send.at[1], w_recv.at[1]).wait_send()
     for b in range(2):
-        all_of(cr.at[b, 0:15], c_send.at[b], c_recv.at[b]).wait_send()
+        all_of(cr.at[b], c_send.at[b], c_recv.at[b]).wait_send()
     for g, (lo, hi, first, last) in enumerate(groups):
-        all_of(mg.at[max(lo, 1) : hi], e_send.at[g], e_recv.at[g]).wait_send()
+        all_of(mg.at[lo:hi], e_send.at[g], e_recv.at[g]).wait_send()
         all_of(xw.at[0:15, lo:hi], f_send.at[g], f_recv.at[g]).wait_send()
 
     @pl.when(t == z)
@@ -441,6 +443,7 @@
             pltpu.VMEM((2, 3, 64, 128), F32),
             pltpu.VMEM((2, 16, 8, 128), BF16),
             pltpu.VMEM((2, 16, 8, 128), BF16),
+            pltpu.VMEM((2, 16, 8, 128), BF16),
             pltpu.VMEM((16, 40, 128), F32),
             pltpu.VMEM((2, 16, 40, 128), BF16),
             pltpu.VMEM((2, 16, 40, 128), BF16),

time: 63.9 us -> 65.1 us (1.019)
  the two profiles are of different devices: /device:TPU:17 before, /device:TPU:13 now
where the time goes in v6:
time: 65.1 us; the launch traced here: 65 us
  Pallas kernels  63 us (97%)
  local copies, waits for them, and re-layouts  1.34 us (2%)
    pallas_call x1, Pallas kernels, shards(): pl.pallas_call(kernel, out_shape=(pltpu.VMEM((12, 128), BF16), pltpu.VMEM...  63 us
    unnamed x2, local copies, waits for them, and re-layouts  1.34 us

profile of v6, /device:TPU:13, one launch (start us, length us, event | category | flops | bytes accessed | tf_op | source)
XLA Modules:
  0.0 65.0 jit_solution(14221745125793600065)
XLA Ops:
  0.6 63.0 %shard_map.149 = (bf16[12,128]{1,0:T(8,128)(2,1)S(1)}, f32[2,3,2,64,64]{4,3,2,1,0:T(8,128)S(1)}) custom-call(bf16[12,128]{1,0:T(8,128)(2,1)} %x_hbm.1, s32[3]{0:T(128)} %live_hbm.1, bf16[2,128]{1,0:T(2,128)(2,1)} %gain_hbm.1, bf16[2,128,128]{2,1,0:T(8,128)(2,1)} %wq.1, bf16[2,128,128]{2,1,0:T(8,128)(2,1)} %wk.1, bf16[2,128,128]{2,1,0:T(8,128)(2,1)} %wv.1, ...), custom_call_target="tpu_custom_call" | custom-call | tf_op jit(solution)/shard_map/pallas_call | solution.py:422
  63.6 0.6 copy.18
  64.2 0.7 %copy.19 = f32[2,3,2,64,64]{4,3,2,1,0:T(8,128)} copy(f32[2,3,2,64,64]{4,3,2,1,0:T(8,128)S(1)} %get-tuple-element.3) | data formatting | bytes 393216

commit v7 on v3

--- a/solution.py
+++ b/solution.py
@@ -11,6 +11,11 @@
 TP = 16
 NZ = 16
 NEAR = 4
+SIDE = 4
+AROUND = sorted(
+    ((i, j) for i in range(SIDE) for j in range(SIDE) if i + j > 0),
+    key=lambda at: -min(at[0], SIDE - at[0]) - min(at[1], SIDE - at[1]),
+)
 WIDTH = 2048
 F32 = jnp.float32
 BF16 = jnp.bfloat16
@@ -40,29 +45,33 @@
     past_half = away // 9
     slot_here = (1 - past_half) * (2 * away - (away + 15) // 16) + past_half * (32 - 2 * away)
 
+    load_rows = pltpu.make_async_copy(x_hbm, xin, load_sem.at[0])
+    load_rows.start()
     barrier = pltpu.get_barrier_semaphore()
 
-    def greet_plane(r, carry):
-        to = (t + r) % TP
-        pl.semaphore_signal(barrier, inc=1, device_id=(to, z * 2), device_id_type=MESH)
-        pl.semaphore_signal(barrier, inc=1, device_id=(to, z * 2 + 1), device_id_type=MESH)
-        return carry
+    y = t // SIDE
+    x = t % SIDE
+
+    def in_plane(up, right):
+        return ((y + up) % SIDE) * SIDE + (x + right) % SIDE
 
     def greet_column(r, carry):
         for to in ((z + r) % NZ, (z + NZ - r) % NZ):
             pl.semaphore_signal(barrier, inc=1, device_id=(t, to * 2 + c), device_id_type=MESH)
         return carry
 
-    lax.fori_loop(1, NEAR + 1, greet_column, 0)
-    lax.fori_loop(1, TP, greet_plane, 0)
+    for r in range(NEAR, 0, -1):
+        greet_column(r, 0)
+    for up, right in AROUND:
+        for core in range(2):
+            pl.semaphore_signal(
+                barrier, inc=1, device_id=(in_plane(up, right), z * 2 + core), device_id_type=MESH
+            )
     pl.semaphore_signal(barrier, inc=1, device_id=(t, z * 2 + other), device_id_type=MESH)
 
     mine = pl.ds(pl.multiple_of(c * 128, 128), 128)
     weights = (wq, wk, wv, wf, wl, we)
-    loads = [
-        pltpu.make_async_copy(x_hbm, xin, load_sem.at[0]),
-        pltpu.make_async_copy(live_hbm, live_ref, load_sem.at[14]),
-    ]
+    loads = [pltpu.make_async_copy(live_hbm, live_ref, load_sem.at[14])]
     for p, w in enumerate(weights):
         loads.append(
             pltpu.make_async_copy(w, wcat.at[:, mine, pl.ds(p * 128, 128)], load_sem.at[1 + p])
@@ -89,16 +98,13 @@
     def head_sum(x):
         return jnp.dot(split_two(x), ones_block, preferred_element_type=F32)
 
-    loads[0].wait()
+    load_rows.wait()
     xrows[...] = jnp.zeros((16, 128), F32)
     xrows[0:12, :] = xin[...].astype(F32)
     first = xrows[0:8, :]
     second = xrows[6:14, :]
     xs[0] = first.astype(BF16)
     xs[1] = second.astype(BF16)
-    for copy in loads[1:]:
-        copy.wait()
-
     pl.semaphore_wait(barrier, 2 * (TP - 1) + 1 + 2 * NEAR)
 
     def remote(src, dst, send, recv, to_t, to_z, to_c):
@@ -115,13 +121,9 @@
             xs.at[core], xg.at[c, slot_here], a_send, a_recv, to, z, core
         )
 
-    def row_step(r, carry):
-        to = (t + r) % TP
-        row_copy(to, 0).start()
-        row_copy(to, 1).start()
-        return carry
-
-    lax.fori_loop(1, TP, row_step, 0)
+    for up, right in AROUND:
+        row_copy(in_plane(up, right), 0).start()
+        row_copy(in_plane(up, right), 1).start()
     row_copy(t, other).start()
     for to in ((z + NEAR) % NZ, (z + NZ - NEAR) % NZ):
         pl.semaphore_signal(far_sem, inc=1, device_id=(t, to * 2 + c), device_id_type=MESH)
@@ -133,6 +135,8 @@
         to_sibling(wcat.at[1, mine, :], 2),
         to_sibling(wall0.at[:, :, mine], 3),
     ]
+    for copy in loads:
+        copy.wait()
     swaps[0].start()
     swaps[1].start()
 
@@ -190,7 +194,7 @@
 
         column(start, first, last)
 
-    groups = ((0, 7, 1, 3), (7, 13, 4, 6), (13, 16, 7, 8))
+    groups = ((0, 3, 1, 1), (3, 7, 2, 3), (7, 11, 4, 5), (11, 15, 6, 7), (15, 16, 8, 8))
     for b in range(2):
         if b == 0:
             swaps[0].wait_recv()
@@ -250,8 +254,7 @@
         decay = jnp.exp(fade8 - ceil[b : b + 1, :] * jax.nn.sigmoid(decay_pre))
         rate = jax.nn.sigmoid(rate_pre)
         gate = jax.nn.sigmoid(gate_pre)
-        unit = key * lax.rsqrt(head_sum(key * key) + 1e-06)
-        unit_rate = unit * rate
+        removal = key * rate / (head_sum(key * key) + 1e-06)
         spread = head_sum(
             jnp.concatenate(
                 [jnp.where(diagonal, value[i : i + 1, :], 0.0) for i in range(6)], axis=0
@@ -259,17 +262,18 @@
         )
         memory = [packed[b, s] for s in range(3)]
         readouts = [None] * 6
+        spreads = [None] * 6
         for j in range(2):
             removed = head_sum(
                 jnp.concatenate(
-                    [memory[s] * unit[2 * s + j : 2 * s + j + 1, :] for s in range(3)], axis=0
+                    [memory[s] * key[2 * s + j : 2 * s + j + 1, :] for s in range(3)], axis=0
                 )
             )
             for s in range(3):
                 i = 2 * s + j
                 updated = (
                     memory[s] * decay[i : i + 1, :]
-                    - removed[64 * s : 64 * s + 64] * unit_rate[i : i + 1, :]
+                    - removed[64 * s : 64 * s + 64] * removal[i : i + 1, :]
                     + spread[64 * i : 64 * i + 64] * key[i : i + 1, :]
                 )
                 memory[s] = jnp.where(j < live_ref[s], updated, memory[s])
@@ -279,18 +283,20 @@
                 )
             )
             for s in range(3):
+                here = read_out[64 * s : 64 * s + 64]
+                here = here - jnp.sum(here, axis=0, keepdims=True) * (1.0 / 64.0)
+                spreads[2 * s + j] = jnp.sum(here * here, axis=0, keepdims=True)
                 readouts[2 * s + j] = jnp.sum(
-                    jnp.where(diagonal, read_out[64 * s : 64 * s + 64], 0.0), axis=0, keepdims=True
-                )
-        readout = jnp.concatenate(readouts, axis=0)
-        centered = readout - head_sum(readout) * (1.0 / 64.0)
-        variance = head_sum(centered * centered) * (1.0 / 64.0)
+                    jnp.where(diagonal, here, 0.0), axis=0, keepdims=True
+                )
+        variance = jnp.concatenate(spreads, axis=0) * (1.0 / 64.0)
+        centered = jnp.concatenate(readouts, axis=0)
         normed = centered * lax.rsqrt(variance + GROUP_EPS) * resc[b : b + 1, :]
         mixed = jnp.where(live_rows[0:6], normed * gate, 0.0)
         ms[b] = jnp.concatenate([mixed, jnp.zeros((2, 128), F32)], axis=0).astype(BF16)
 
         if b == 0:
-            for g in (2, 1, 0):
+            for g in (4, 3, 2, 1, 0):
                 lo, hi, first, last = groups[g]
 
                 def start(to, here, there):
@@ -307,7 +313,7 @@
             def start_both(to, here, there):
                 for core in range(2):
                     remote(
-                        ms.at[1], fin.at[c * TP + t], e_send.at[3], e_recv.at[3], z, to, core
+                        ms.at[1], fin.at[c * TP + t], e_send.at[5], e_recv.at[5], z, to, core
                     ).start()
 
             column(start_both, 1, 8)
@@ -315,7 +321,7 @@
             @pl.when(t == z)
             def _():
                 remote(
-                    ms.at[1], fin.at[c * TP + t], e_send.at[3], e_recv.at[3], z, z, other
+                    ms.at[1], fin.at[c * TP + t], e_send.at[5], e_recv.at[5], z, z, other
                 ).start()
                 fin[c * TP + t] = ms[1]
 
@@ -323,7 +329,7 @@
             def _():
                 for core in range(2):
                     remote(
-                        ms.at[1], fin.at[c * TP + t], e_send.at[3], e_recv.at[3], z, z, core
+                        ms.at[1], fin.at[c * TP + t], e_send.at[5], e_recv.at[5], z, z, core
                     ).start()
 
         for s in range(3):
@@ -335,14 +341,11 @@
                 arriving = mg.at[max(lo, 1) : hi]
                 all_of(arriving, e_send.at[g], e_recv.at[g]).wait_recv()
 
-                def forward(r, carry):
+                for up, right in AROUND:
                     remote(
                         mg.at[lo:hi], xw.at[t, lo:hi], f_send.at[g], f_recv.at[g],
-                        (t + r) % TP, z, c,
+                        in_plane(up, right), z, c,
                     ).start()
-                    return carry
-
-                lax.fori_loop(1, TP, forward, 0)
                 xw[t, lo:hi] = mg[lo:hi]
 
     all_of(wall1.at[0:15], w_send.at[1], w_recv.at[1]).wait_recv()
@@ -350,11 +353,11 @@
 
     @pl.when(t == z)
     def _():
-        all_of(fin.at[0:31], e_send.at[3], e_recv.at[3]).wait_recv()
+        all_of(fin.at[0:31], e_send.at[5], e_recv.at[5]).wait_recv()
 
     @pl.when(t != z)
     def _():
-        all_of(fin, e_send.at[3], e_recv.at[3]).wait_recv()
+        all_of(fin, e_send.at[5], e_recv.at[5]).wait_recv()
 
     heads = jnp.concatenate(
         [
@@ -385,11 +388,22 @@
 
     @pl.when(t == z)
     def _():
-        all_of(fin.at[0:31], e_send.at[3], e_recv.at[3]).wait_send()
+        all_of(fin.at[0:31], e_send.at[5], e_recv.at[5]).wait_send()
 
     @pl.when(t != z)
     def _():
-        all_of(fin, e_send.at[3], e_recv.at[3]).wait_send()
+        all_of(fin, e_send.at[5], e_recv.at[5]).wait_send()
+
+
+def store_results(rows_ref, states_ref, rows_out, states_out, sem):
+    copies = [
+        pltpu.make_async_copy(states_ref, states_out, sem.at[0]),
+        pltpu.make_async_copy(rows_ref, rows_out, sem.at[1]),
+    ]
+    for copy in copies:
+        copy.start()
+    for copy in copies:
+        copy.wait()
 
 
 def shards(*arrays):
@@ -398,7 +412,7 @@
     hbm = pl.BlockSpec(memory_space=pltpu.HBM)
     in_specs = [hbm] * 14
     dma = pltpu.SemaphoreType.DMA
-    return pl.pallas_call(
+    results = pl.pallas_call(
         kernel,
         out_shape=(
             pltpu.VMEM((12, 128), BF16),
@@ -438,10 +452,10 @@
             dma,
             dma((2,)),
             dma((2,)),
-            dma((4,)),
-            dma((4,)),
-            dma((3,)),
-            dma((3,)),
+            dma((6,)),
+            dma((6,)),
+            dma((5,)),
+            dma((5,)),
             dma((2,)),
             dma((2,)),
             dma,
@@ -450,6 +464,17 @@
         ],
         compiler_params=pltpu.CompilerParams(collective_id=0, has_side_effects=True, vmem_limit_bytes=24 * 1024 * 1024),
     )(*arrays)
+    return pl.pallas_call(
+        store_results,
+        out_shape=(
+            jax.ShapeDtypeStruct((12, 128), BF16),
+            jax.ShapeDtypeStruct((2, 3, 2, 64, 64), F32),
+        ),
+        in_specs=[pl.BlockSpec(memory_space=pltpu.VMEM)] * 2,
+        out_specs=(hbm, hbm),
+        scratch_shapes=[dma((2,))],
+        compiler_params=pltpu.CompilerParams(vmem_limit_bytes=1024 * 1024),
+    )(*results)
 
 
 def solution(mesh):

time: 62.4 us -> 61.4 us (0.984)
  local copies, waits for them, and re-layouts: 1.34 us -> 0 us
    unnamed x2 -> x0, local copies, waits for them, and re-layouts: 1.34 us -> none
    pallas_call x0 -> x1, Pallas kernels: none -> 0.77 us  [shards(): pl.pallas_call(store_results, out_shape=(jax.ShapeDtypeStruct((12, 128),...]
where the time goes in v7:
time: 61.4 us; the launch traced here: 61.3 us
  Pallas kernels  60.6 us (99%)
  between operations  0.64 us (1%)
    pallas_call x1, Pallas kernels, shards(): pl.pallas_call(kernel, out_shape=(pltpu.VMEM((12, 128), BF16), pltpu.VMEM...  59.9 us

profile of v7, /device:TPU:17, one launch (start us, length us, event | category | flops | bytes accessed | tf_op | source)
XLA Modules:
  0.0 61.3 jit_solution(2622879472892021293)
XLA Ops:
  0.6 59.9 %shard_map.149 = (bf16[12,128]{1,0:T(8,128)(2,1)S(1)}, f32[2,3,2,64,64]{4,3,2,1,0:T(8,128)S(1)}) custom-call(bf16[12,128]{1,0:T(8,128)(2,1)} %x_hbm.1, s32[3]{0:T(128)} %live_hbm.1, bf16[2,128]{1,0:T(2,128)(2,1)} %gain_hbm.1, bf16[2,128,128]{2,1,0:T(8,128)(2,1)} %wq.1, bf16[2,128,128]{2,1,0:T(8,128)(2,1)} %wk.1, bf16[2,128,128]{2,1,0:T(8,128)(2,1)} %wv.1, ...), custom_call_target="tpu_custom_call" | custom-call | tf_op jit(solution)/shard_map/pallas_call | solution.py:415
  60.5 0.8 %shard_map.150 = (bf16[12,128]{1,0:T(8,128)(2,1)}, f32[2,3,2,64,64]{4,3,2,1,0:T(8,128)}) custom-call(bf16[12,128]{1,0:T(8,128)(2,1)S(1)} %get-tuple-element.4.rows_ref, f32[2,3,2,64,64]{4,3,2,1,0:T(8,128)S(1)} %get-tuple-element.5.states_ref), custom_call_target="tpu_custom_call" | custom-call | tf_op jit(solution)/shard_map/pallas_call | solution.py:467

commit v8 on v7

--- a/solution.py
+++ b/solution.py
@@ -11,6 +11,7 @@
 TP = 16
 NZ = 16
 NEAR = 4
+SENT = 38
 SIDE = 4
 AROUND = sorted(
     ((i, j) for i in range(SIDE) for j in range(SIDE) if i + j > 0),
@@ -135,10 +136,12 @@
         to_sibling(wcat.at[1, mine, :], 2),
         to_sibling(wall0.at[:, :, mine], 3),
     ]
-    for copy in loads:
+    for copy in loads[1:7] + loads[9:10]:
         copy.wait()
     swaps[0].start()
     swaps[1].start()
+    for copy in loads[0:1] + loads[7:9] + loads[10:]:
+        copy.wait()
 
     def exit_step(r, carry):
         mine_here = wall0.at[t, :, mine]
@@ -178,9 +181,13 @@
         )
         squares = jnp.sum(rows[0] * rows[0] + rows[1] * rows[1], axis=1, keepdims=True)
         squares = jnp.broadcast_to(squares, (count, 128)).reshape(hi - lo, 8, 128)
-        lower = lax.broadcasted_iota(jnp.int32, (hi - lo, 3, 128), 2) < 64
+        token_at = lax.broadcasted_iota(jnp.int32, (hi - lo, 8, 128), 1)
+        place_at = lax.broadcasted_iota(jnp.int32, (hi - lo, 8, 128), 2) // 16
+        line = jnp.sum(jnp.where(token_at == place_at, squares, 0.0), axis=1, keepdims=True)
+        rounded = line.astype(BF16).astype(F32)
         acc[lo:hi, 36:40, :] = jnp.zeros((hi - lo, 4, 128), F32)
-        acc[lo:hi, 36:39, :] = jnp.where(lower, squares[:, 0:3], squares[:, 3:6])
+        acc[lo:hi, 36:37, :] = rounded
+        acc[lo:hi, 37:38, :] = line - rounded
         for p in range(6):
             part = jnp.dot(
                 gained, wcat[b, :, p * 128 : (p + 1) * 128], preferred_element_type=F32
@@ -190,7 +197,7 @@
 
     def send_partials(b, first, last):
         def start(to, here, there):
-            remote(cs.at[b, here], cr.at[b, z], c_send.at[b], c_recv.at[b], t, to, c).start()
+            remote(cs.at[b, here, 0:SENT], cr.at[b, z, 0:SENT], c_send.at[b], c_recv.at[b], t, to, c).start()
 
         column(start, first, last)
 
@@ -241,12 +248,12 @@
         live_rows = (row8 % 2) < live8
         fade8 = jnp.where(low_half[0:6], fade_columns[:, 2 * b : 2 * b + 1], fade_columns[:, 2 * b + 1 : 2 * b + 2])
 
-        all_of(cr.at[b, 0:15], c_send.at[b], c_recv.at[b]).wait_recv()
+        all_of(cr.at[b, 0:15, 0:SENT], c_send.at[b], c_recv.at[b]).wait_recv()
         summed[0:40, :] = jnp.sum(cr[b].astype(F32), axis=0)
-        square_rows = summed[36:39, :]
-        low_squares = square_rows[:, 0:1]
-        high_squares = square_rows[:, 64:65]
-        token_squares = jnp.concatenate([low_squares, high_squares], axis=0)
+        line = summed[36:37, :] + summed[37:38, :]
+        token_squares = jnp.sum(
+            jnp.where(row8[0:6] == lane[0:6] // 16, line, 0.0), axis=1, keepdims=True
+        ) * (1.0 / 16.0)
         row_scale = lax.rsqrt(token_squares / D + NORM_EPS)
         read, key, value, decay_pre, rate_pre, gate_pre = [
             summed[p * 6 : p * 6 + 6, :] * row_scale for p in range(6)
@@ -381,7 +388,7 @@
     all_of(wall0.at[0:15, :, mine], w_send.at[0], w_recv.at[0]).wait_send()
     all_of(wall1.at[0:15], w_send.at[1], w_recv.at[1]).wait_send()
     for b in range(2):
-        all_of(cr.at[b, 0:15], c_send.at[b], c_recv.at[b]).wait_send()
+        all_of(cr.at[b, 0:15, 0:SENT], c_send.at[b], c_recv.at[b]).wait_send()
     for g, (lo, hi, first, last) in enumerate(groups):
         all_of(mg.at[max(lo, 1) : hi], e_send.at[g], e_recv.at[g]).wait_send()
         all_of(xw.at[0:15, lo:hi], f_send.at[g], f_recv.at[g]).wait_send()

time: 61.4 us -> 61.2 us (level)
  no operation moved by 1% of the time
where the time goes in v8:
time: 61.2 us; the launch traced here: 61.1 us
  Pallas kernels  60.4 us (99%)
  between operations  0.64 us (1%)
    pallas_call x1, Pallas kernels, shards(): pl.pallas_call(kernel, out_shape=(pltpu.VMEM((12, 128), BF16), pltpu.VMEM...  59.7 us

profile of v8, /device:TPU:17, one launch (start us, length us, event | category | flops | bytes accessed | tf_op | source)
XLA Modules:
  0.0 61.1 jit_solution(9278197700508868752)
XLA Ops:
  0.6 59.7 %shard_map.149 = (bf16[12,128]{1,0:T(8,128)(2,1)S(1)}, f32[2,3,2,64,64]{4,3,2,1,0:T(8,128)S(1)}) custom-call(bf16[12,128]{1,0:T(8,128)(2,1)} %x_hbm.1, s32[3]{0:T(128)} %live_hbm.1, bf16[2,128]{1,0:T(2,128)(2,1)} %gain_hbm.1, bf16[2,128,128]{2,1,0:T(8,128)(2,1)} %wq.1, bf16[2,128,128]{2,1,0:T(8,128)(2,1)} %wk.1, bf16[2,128,128]{2,1,0:T(8,128)(2,1)} %wv.1, ...), custom_call_target="tpu_custom_call" | custom-call | tf_op jit(solution)/shard_map/pallas_call | solution.py:422
  60.3 0.8 %shard_map.150 = (bf16[12,128]{1,0:T(8,128)(2,1)}, f32[2,3,2,64,64]{4,3,2,1,0:T(8,128)}) custom-call(bf16[12,128]{1,0:T(8,128)(2,1)S(1)} %get-tuple-element.4.rows_ref, f32[2,3,2,64,64]{4,3,2,1,0:T(8,128)S(1)} %get-tuple-element.5.states_ref), custom_call_target="tpu_custom_call" | custom-call | tf_op jit(solution)/shard_map/pallas_call | solution.py:474

commit v9 on v8

--- a/solution.py
+++ b/solution.py
@@ -208,9 +208,11 @@
             swaps[1].wait_recv()
             all_of(fin.at[0:31], a_send, a_recv).wait_recv()
             rows = [xg[h].astype(F32).reshape(128, 128) for h in range(2)]
-            project(0, rows, 0, 16)
-            pl.semaphore_wait(far_sem, 2)
-            send_partials(0, 1, 8)
+            for lo, hi, first, last in ((7, 16, 4, 8), (0, 7, 1, 3)):
+                project(0, [row[8 * lo : 8 * hi] for row in rows], lo, hi)
+                if last == 8:
+                    pl.semaphore_wait(far_sem, 2)
+                send_partials(0, first, last)
             lax.fori_loop(1, TP, exit_step, 0)
         else:
             swaps[2].wait_recv()

time: 61.2 us -> 61.2 us (level)
  no operation moved by 1% of the time
where the time goes in v9:
time: 61.2 us; the launch traced here: 61.1 us
  Pallas kernels  60.5 us (99%)
  between operations  0.64 us (1%)
    pallas_call x1, Pallas kernels, shards(): pl.pallas_call(kernel, out_shape=(pltpu.VMEM((12, 128), BF16), pltpu.VMEM...  59.7 us

profile of v9, /device:TPU:17, one launch (start us, length us, event | category | flops | bytes accessed | tf_op | source)
XLA Modules:
  0.0 61.1 jit_solution(17784668872864745179)
XLA Ops:
  0.6 59.7 %shard_map.149 = (bf16[12,128]{1,0:T(8,128)(2,1)S(1)}, f32[2,3,2,64,64]{4,3,2,1,0:T(8,128)S(1)}) custom-call(bf16[12,128]{1,0:T(8,128)(2,1)} %x_hbm.1, s32[3]{0:T(128)} %live_hbm.1, bf16[2,128]{1,0:T(2,128)(2,1)} %gain_hbm.1, bf16[2,128,128]{2,1,0:T(8,128)(2,1)} %wq.1, bf16[2,128,128]{2,1,0:T(8,128)(2,1)} %wk.1, bf16[2,128,128]{2,1,0:T(8,128)(2,1)} %wv.1, ...), custom_call_target="tpu_custom_call" | custom-call | tf_op jit(solution)/shard_map/pallas_call | solution.py:424
  60.3 0.8 %shard_map.150 = (bf16[12,128]{1,0:T(8,128)(2,1)}, f32[2,3,2,64,64]{4,3,2,1,0:T(8,128)}) custom-call(bf16[12,128]{1,0:T(8,128)(2,1)S(1)} %get-tuple-element.4.rows_ref, f32[2,3,2,64,64]{4,3,2,1,0:T(8,128)S(1)} %get-tuple-element.5.states_ref), custom_call_target="tpu_custom_call" | custom-call | tf_op jit(solution)/shard_map/pallas_call | solution.py:476
